TPU v7x, 512 devices: a 4x2x32 block of a 4x8x32 slice. The times are simulated.
512 devices in a mesh: grp: 2 (over y), fs: 32 (over z), tp: 8 (over x, core).
Axes of the slice: x: 4, y: 2, z: 32, core: 2. Of those that a mesh axis runs over, the one named last changes fastest.
The devices are a block of a 4x8x32 slice.
Arguments:
- prompt: bfloat16 [4096, 2048], P(('grp', 'tp')), parts along dimension 0, may hold values from -6 to 6
- gain_first: float32 [2048], P('fs'), may hold values from 0.1 to 1.9
- gate_first: float32 [2048, 4096], P('fs', 'tp'), may hold values from -0.125 to 0.125
- up_first: float32 [2048, 4096], P('fs', 'tp'), may hold values from -0.125 to 0.125
- down_first: float32 [4096, 2048], P('fs', 'tp'), may hold values from -0.09375 to 0.09375
- gain_second: float32 [2048], P('fs'), may hold values from 0.1 to 1.9
- gate_second: float32 [2048, 4096], P('fs', 'tp'), may hold values from -0.125 to 0.125
- up_second: float32 [2048, 4096], P('fs', 'tp'), may hold values from -0.125 to 0.125
- down_second: float32 [4096, 2048], P('fs', 'tp'), may hold values from -0.09375 to 0.09375
Outputs:
- result: bfloat16 [4096, 2048], P(('grp', 'tp')), parts along dimension 0
- served_gate_first: bfloat16 [4096, 4096], P('grp', 'fs'), parts along dimension 0
- served_up_first: bfloat16 [4096, 4096], P('grp', 'fs'), parts along dimension 0
- served_down_first: bfloat16 [4096, 4096], P('fs', 'grp'), parts along dimension 1
- served_gate_second: bfloat16 [4096, 4096], P('grp', 'fs'), parts along dimension 0
- served_up_second: bfloat16 [4096, 4096], P('grp', 'fs'), parts along dimension 0
- served_down_second: bfloat16 [4096, 4096], P('fs', 'grp'), parts along dimension 1
There are 2 independent parts, one for each index of `grp`. A program takes and returns all parts, laid end to end along the dimension named above; an argument that names none is the same for every part. Nothing has to cross between parts.
All inputs are finite; a program needn't handle non-finite values.
Results may differ from a plain program's by a relative error of at most 0.0053.
Values may be sent and summed in bfloat16 or wider, within the bound.
No kernel may reach another device: no remote copies, remote signals or barrier semaphores. Data moves between devices by JAX's collectives and lax.ppermute only.
A program may use at most 64 MiB of HBM per device.

v0:
```python
import jax
import jax.numpy as jnp
from jax import lax
from jax.experimental import pallas as pl
from jax.experimental.layout import Layout, with_layout_constraint
from jax.experimental.pallas import tpu as pltpu
from jax.sharding import PartitionSpec as P


EPS = 1e-06
NEAR = 4
BF16 = jnp.bfloat16


def fold(gain, weight):
    return (gain[:, None] * weight).astype(BF16)


def normed_of(stream):
    return (stream * lax.rsqrt(jnp.mean(stream * stream, axis=-1, keepdims=True) + EPS)).astype(BF16)


def row_major(array):
    return with_layout_constraint(array, Layout(major_to_minor=tuple(range(array.ndim))))


def exchange(blocks, axis, groups=None):
    return lax.all_to_all(blocks, axis, split_axis=0, concat_axis=0, tiled=True, axis_index_groups=groups)


def spread_copies(array, axis, members, groups=None):
    copies = jnp.broadcast_to(array, (members, *array.shape))
    if groups is not None and len(groups[0]) > members:
        copies = copies.reshape(len(groups[0]), *array.shape[1:])
    return exchange(copies, axis, groups)


def far_groups(n):
    return [list(range(i, n, NEAR)) for i in range(NEAR)]


def chip_groups(n):
    return [list(range(c, n, 2)) for c in range(2)]


def gather_tp(array):
    n = lax.axis_size("tp")
    mine = spread_copies(array, "tp", n // 2, chip_groups(n))
    other = lax.ppermute(mine, "tp", [(i, i ^ 1) for i in range(n)])
    even = lax.axis_index("tp") % 2 == 0
    both = jnp.stack([jnp.where(even, mine, other), jnp.where(even, other, mine)], axis=1)
    return both.reshape(n, *array.shape)


def shift_tp(array, steps):
    n = lax.axis_size("tp")
    return lax.ppermute(array, "tp", [(i, (i + steps) % n) for i in range(n)])


def gather_tp_beside(array):
    n = lax.axis_size("tp")
    chips = n // 2
    me = lax.axis_index("tp")
    mine = jnp.zeros((chips, *array.shape), array.dtype)
    for d in range(chips):
        piece = array if d == 0 else shift_tp(array, -2 * d)
        mine = lax.dynamic_update_index_in_dim(mine, piece, (me // 2 + d) % chips, 0)
    other = lax.ppermute(mine, "tp", [(i, i ^ 1) for i in range(n)])
    even = me % 2 == 0
    both = jnp.stack([jnp.where(even, mine, other), jnp.where(even, other, mine)], axis=1)
    return both.reshape(n, *array.shape)


def shift(array, steps):
    n = lax.axis_size("fs")
    return lax.ppermute(array, "fs", [(i, (i + steps) % n) for i in range(n)])


def part_of(blocks, index, axis=0):
    return lax.dynamic_index_in_dim(blocks, index % blocks.shape[axis], axis, keepdims=False)


def scatter_sum(partial):
    n = lax.axis_size("fs")
    me = lax.axis_index("fs")
    far = n // NEAR
    rows = partial.shape[0] // n
    width = partial.shape[1]
    f32 = jnp.float32

    blocks = partial.astype(BF16).reshape(far, NEAR, rows, width)
    keep, ahead, across, behind = (part_of(blocks, me + d, 1) for d in range(NEAR))
    h = far // 2
    ahead, behind = shift(ahead, 1), shift(behind, -1)
    low, high = shift(across[:h], 2), shift(across[h:], -2)
    total = keep.astype(f32) + ahead.astype(f32) + behind.astype(f32)
    total = total + jnp.concatenate([low, high], axis=0).astype(f32)

    got = exchange(total.astype(BF16), "fs", far_groups(n))
    return jnp.sum(got.astype(f32), axis=0)


def spread_far(own):
    n = lax.axis_size("fs")
    return spread_copies(own, "fs", n // NEAR, far_groups(n))


def gather_near(got):
    n = lax.axis_size("fs")
    me = lax.axis_index("fs")
    far, rows, width = got.shape
    h = far // 2
    ahead, behind = shift(got, -1), shift(got, 1)
    low, high = shift(got[:h], 2), shift(got[h:], -2)
    out = jnp.zeros((far, NEAR, rows, width), got.dtype)
    pieces = (got, ahead, jnp.concatenate([low, high], axis=0), behind)
    for d, piece in enumerate(pieces):
        out = lax.dynamic_update_index_in_dim(out, piece, (me + d) % NEAR, 1)
    return out.reshape(n * rows, width)


def cast_in_plane(whole, rows):
    n, n_tp = lax.axis_size("fs"), lax.axis_size("tp")
    chips = n_tp // 2
    per = n // n_tp
    me, t = lax.axis_index("fs"), lax.axis_index("tp")
    planes, _, cols = whole.shape
    lanes = cols * 2 // per
    home = me // per
    ahead = (t // 2 - home // 2) % chips

    def at(f, steps, core):
        return f * n_tp + 2 * ((f // per // 2 + steps) % chips) + core

    def hop(array, pairs):
        return lax.ppermute(array, ("fs", "tp"), [pair for f in range(n) for pair in pairs(f)])

    def first():
        both = whole[:, : 4 * rows].reshape(planes, 2, 2, rows, cols)
        both = jnp.where(me % per // 2 == 0, both[:, :, 0], both[:, :, 1])
        both = jnp.where(me % 2 == 0, both[..., :lanes], both[..., lanes:])
        return both.transpose(1, 0, 2, 3).reshape(2, planes * rows, lanes)

    def second(array):
        other = hop(array, lambda f: [(f * n_tp + f // per, f * n_tp + (f // per ^ 1))])
        return lambda: jnp.where(t == home, array, other)

    def third(array):
        up = hop(array, lambda f: [(at(f, 0, c), at(f, 1, c)) for c in range(2)])
        down = hop(array, lambda f: [(at(f, 0, c), at(f, -1, c)) for c in range(2)])
        return lambda: jnp.where(ahead == 0, array, jnp.where(ahead == 1, up, down))

    def fourth(array):
        gate = hop(array[0], lambda f: [(at(f, 1, c), at(f, 2, c)) for c in range(2)])
        up = hop(array[1], lambda f: [(at(f, -1, c), at(f, -2, c)) for c in range(2)])
        return lambda: (jnp.where(ahead == 2, gate, array[0]), jnp.where(ahead == 2, up, array[1]))

    return first, second, third, fourth


STEPS = 4


def hidden_kernel(normed, whole):
    tokens, width = normed.shape
    planes, _, cols = whole.shape
    rows = width // planes
    halves = 2
    per = planes // STEPS
    group = 256 // rows

    def body(x_ref, w_ref, o_ref, acc_ref):
        step = pl.program_id(0)

        @pl.when(step == 0)
        def _():
            acc_ref[...] = jnp.zeros_like(acc_ref)

        for j in range(per // group):
            x = x_ref[:, j * group * rows : (j + 1) * group * rows]
            for m in range(2 * halves):
                w = jnp.concatenate(
                    [w_ref[j * group + k, m * rows : (m + 1) * rows, :] for k in range(group)], axis=0
                )
                acc_ref[m] += jnp.dot(x, w, preferred_element_type=jnp.float32)

        @pl.when(step == STEPS - 1)
        def _():
            for m in range(halves):
                gate, up = acc_ref[m], acc_ref[halves + m]
                o_ref[:, m * cols : (m + 1) * cols] = (gate / (1.0 + jnp.exp(-gate)) * up).astype(BF16)

    return pl.pallas_call(
        body,
        grid=(STEPS,),
        in_specs=[
            pl.BlockSpec((tokens, width // STEPS), lambda i: (0, i)),
            pl.BlockSpec((per, 2 * halves * rows, cols), lambda i: (i, 0, 0)),
        ],
        out_specs=pl.BlockSpec((tokens, halves * cols), lambda i: (0, 0)),
        out_shape=jax.ShapeDtypeStruct((tokens, halves * cols), BF16),
        scratch_shapes=[pltpu.VMEM((2 * halves, tokens, cols), jnp.float32)],
        name="hidden_second",
    )(normed, whole)


def down_kernel(hidden, whole, hid):
    n_tp, tokens, cols = hidden.shape
    planes, rows, width = whole.shape
    per = planes // STEPS
    blocks = n_tp // STEPS
    each = per // blocks

    def body(h_ref, w_ref, o_ref):
        step = pl.program_id(0)

        @pl.when(step == 0)
        def _():
            o_ref[...] = jnp.zeros_like(o_ref)

        for b in range(blocks):
            w = w_ref[b * each : (b + 1) * each].reshape(cols, width)
            o_ref[...] += jnp.dot(h_ref[b], w, preferred_element_type=jnp.float32)

    return pl.pallas_call(
        body,
        grid=(STEPS,),
        in_specs=[
            pl.BlockSpec((blocks, tokens, cols), lambda i: (i, 0, 0)),
            pl.BlockSpec((per, hid, width), lambda i: (i, rows // hid - 1, 0)),
        ],
        out_specs=pl.BlockSpec((tokens, width), lambda i: (0, 0)),
        out_shape=jax.ShapeDtypeStruct((tokens, width), jnp.float32),
        name="down_second",
    )(hidden, whole)


def on_device(
    prompt,
    gain_first,
    gate_first,
    up_first,
    down_first,
    gain_second,
    gate_second,
    up_second,
    down_second,
):
    n_fs = lax.axis_size("fs")
    n_tp = lax.axis_size("tp")
    rows, cols = gate_first.shape
    hid, dcols = down_first.shape
    width = prompt.shape[1]
    half = cols // dcols

    g1, u1 = fold(gain_first, gate_first), fold(gain_first, up_first)
    g2, u2 = fold(gain_second, gate_second), fold(gain_second, up_second)
    d1, d2 = down_first.astype(BF16), down_second.astype(BF16)

    pack = [m[:, k * dcols : (k + 1) * dcols] for m in (g2, u2) for k in range(half)] + [d2]
    whole = lax.all_gather(row_major(jnp.concatenate(pack, axis=0)), "fs", axis=0, tiled=True)
    whole = row_major(whole).reshape(n_fs, 2 * half * rows + hid, dcols)

    r = rows // n_tp
    lanes = cols * n_tp // n_fs
    per = n_fs // n_tp
    mats = jnp.stack([g1, u1]).reshape(2, n_tp, r, cols).transpose(1, 0, 2, 3)
    mats = exchange(mats, "tp")
    mats = mats.reshape(n_tp, 2, r, per, lanes).transpose(0, 3, 1, 2, 4).reshape(n_fs, 2, r, lanes)
    mats, d1, d2 = lax.optimization_barrier((mats, d1, d2))
    mats = exchange(mats, "fs")

    def in_lanes(down):
        return [down[:, k * lanes : (k + 1) * lanes] for k in range(dcols // lanes)]

    def pair_of(got):
        pair = got.reshape(n_tp, n_fs, 2, r, lanes).transpose(2, 1, 0, 3, 4).reshape(2, width, lanes)
        return pair[0], pair[1]

    def down_of(got):
        down = got.reshape(n_tp, dcols // lanes, hid, lanes)
        return down.transpose(2, 0, 1, 3).reshape(hid, width)

    downs = jnp.concatenate([*in_lanes(d1), *in_lanes(d2)], axis=0)
    downs = gather_tp_beside(downs)
    mats, downs = lax.optimization_barrier((mats, downs))
    cut = dcols // lanes * hid
    first = (*pair_of(gather_tp(mats.reshape(-1, lanes))), down_of(downs[:, :cut]))
    down_second_served = down_of(downs[:, cut:])

    stream = prompt.astype(jnp.float32)
    normed = normed_of(stream)
    gate = jnp.dot(normed, first[0], preferred_element_type=jnp.float32)
    up = jnp.dot(normed, first[1], preferred_element_type=jnp.float32)
    hidden = (jax.nn.silu(gate) * up).astype(BF16)
    partial = jnp.dot(hidden, first[2], preferred_element_type=jnp.float32)
    tokens = prompt.shape[0] // n_fs
    own = lax.dynamic_slice_in_dim(prompt, lax.axis_index("fs") * tokens, tokens, 0).astype(jnp.float32)
    own = own + 0.5 * scatter_sum(partial)

    normed = spread_copies(normed_of(own), "tp", n_tp).reshape(n_tp * tokens, width)
    hidden = hidden_kernel(normed, whole)
    step1, step2, step3, step4 = cast_in_plane(whole, rows)
    hidden = spread_copies(hidden, "tp", n_tp)
    cast = step1()
    done = step2(cast)
    out = down_kernel(hidden, whole, hid)
    out = exchange(out.reshape(n_tp, tokens, dcols), "tp")
    cast = done()
    done = step3(cast)
    own = own + 0.5 * out.transpose(1, 0, 2).reshape(tokens, width)
    got = spread_far(own.astype(BF16))
    cast = done()
    done = step4(cast)
    gate_served, up_served = done()
    result = gather_near(got)
    return (result, first[0], first[1], first[2], gate_served, up_served, down_second_served)


def solution(mesh):
    return jax.shard_map(
        on_device,
        mesh=mesh,
        in_specs=(
            P(("grp", "tp"), None),
            P("fs"),
            P("fs", "tp"),
            P("fs", "tp"),
            P("fs", "tp"),
            P("fs"),
            P("fs", "tp"),
            P("fs", "tp"),
            P("fs", "tp"),
        ),
        out_specs=(
            P(("grp", "tp"), None),
            P("grp", "fs"),
            P("grp", "fs"),
            P("fs", "grp"),
            P("grp", "fs"),
            P("grp", "fs"),
            P("fs", "grp"),
        ),
        check_vma=False,
    )
```

profile of v0, /device:TPU:44, one launch (start us, length us, event | category | flops | bytes accessed | tf_op | source)
XLA Modules:
  0.0 361.0 jit_solution(10981125998483720986)
XLA Ops:
  7.3 1.1 multiply_convert_fusion
  10.0 1.1 fusion.18
  11.8 4.8 %all-to-all-start = ((bf16[8,2,8,512]{3,2,1,0:T(8,128)(2,1)}), bf16[8,2,8,512]{3,2,1,0:T(8,128)(2,1)S(1)}, u32[]{:S(2)}, u32[]{:S(2)}) async-start(bf16[8,2,8,512]{3,2,1,0:T(8,128)(2,1)} %maximum_bitcast_fusion.1), calls=%async_computation | async-start | bytes 262144 | tf_op jit(solution)/shard_map/all_to_all | solution.py:28
  16.6 3.4 all-to-all-done
  20.7 3.8 %collective-permute-start = (bf16[512,128]{1,0:T(8,128)(2,1)S(1)}, bf16[512,128]{1,0:T(8,128)(2,1)S(1)}, u32[]{:S(2)}, u32[]{:S(2)}) collective-permute-start(bf16[512,128]{1,0:T(8,128)(2,1)S(1)} %pad_maximum_fusion.3), channel_id=1, source_target_pairs={{0,6},{1,7},{2,0},{3,1},{4,2},{5,3},{6,4},{7,5},{8,14},{9,15},{10,... | collective-permute-start | bytes 393224 | tf_op jit(solution)/shard_map/ppermute | solution.py:57
  24.6 4.0 %collective-permute-start.1 = (bf16[512,128]{1,0:T(8,128)(2,1)S(1)}, bf16[512,128]{1,0:T(8,128)(2,1)S(1)}, u32[]{:S(2)}, u32[]{:S(2)}) collective-permute-start(bf16[512,128]{1,0:T(8,128)(2,1)S(1)} %pad_maximum_fusion.3), channel_id=1, source_target_pairs={{0,4},{1,5},{2,6},{3,7},{4,0},{5,1},{6,2},{7,3},{8,12},{9,13},{10,... | collective-permute-start | bytes 393224 | tf_op jit(solution)/shard_map/ppermute | solution.py:57
  28.6 3.4 collective-permute-start.2
  32.0 45.8 %all-to-all-start.1 = ((bf16[32,2,8,128]{3,2,1,0:T(8,128)(2,1)}), bf16[32,2,8,128]{3,2,1,0:T(8,128)(2,1)S(1)}, u32[]{:S(2)}, u32[]{:S(2)}) async-start(bf16[32,2,8,128]{3,2,1,0:T(8,128)(2,1)} %bitcast.3), calls=%async_computation.1 | async-start | bytes 262144 | tf_op jit(solution)/shard_map/all_to_all | solution.py:28
  78.0 2.0 collective-permute-start.3
  80.0 1.9 collective-permute-done.3
  82.1 27.9 %all-to-all-done.1 = bf16[32,2,8,128]{3,2,1,0:T(8,128)(2,1)S(1)} async-done(((bf16[32,2,8,128]{3,2,1,0:T(8,128)(2,1)}), bf16[32,2,8,128]{3,2,1,0:T(8,128)(2,1)S(1)}, u32[]{:S(2)}, u32[]{:S(2)}) %all-to-all-start.1) | async-done | bytes 131104 | tf_op jit(solution)/shard_map/all_to_all | solution.py:28
  110.0 10.0 %all_to_all.40 = bf16[4,512,128]{2,1,0:T(8,128)(2,1)S(1)} all-to-all(bf16[4,512,128]{2,1,0:T(8,128)(2,1)S(1)} %broadcast_in_dim.56), channel_id=1, replica_groups={{0,2,4,6},{1,3,5,7},{8,10,12,14},{9,11,13,15},{16,18,20,22},{17,19,21,2..., dimensions={0} | all-to-all | bytes 1048576 | tf_op jit(solution)/shard_map/all_to_all | solution.py:28
  120.0 1.9 collective-permute-start.4
  124.0 1.1 select_bitcast_fusion.1
  128.1 2.1 collective-permute-start.5
  130.2 5.0 %collective-permute-start.6 = (bf16[8,8,2048]{2,1,0:T(8,128)(2,1)S(1)}, bf16[8,8,2048]{2,1,0:T(8,128)(2,1)S(1)}, u32[]{:S(2)}, u32[]{:S(2)}) collective-permute-start(bf16[8,8,2048]{2,1,0:T(8,128)(2,1)S(1)} %get-tuple-element.33), channel_id=1, source_target_pairs={{0,248},{8,0},{16,8},{24,16},{32,24},{40,32},{48,40},{56,48},{64,5... | collective-permute-start | bytes 786440 | tf_op jit(solution)/shard_map/ppermute | solution.py:76
  135.9 1.9 collective-permute-start.7
  138.5 6.1 %collective-permute-start.8 = (bf16[4,8,2048]{2,1,0:T(8,128)(2,1)}, bf16[4,8,2048]{2,1,0:T(8,128)(2,1)}, u32[]{:S(2)}, u32[]{:S(2)}) collective-permute-start(bf16[4,8,2048]{2,1,0:T(8,128)(2,1)} %dynamic-slice_bitcast_fusion.3), channel_id=1, source_target_pairs={{0,240},{8,248},{16,0},{24,8},{32,16},{40,24},{48,32},{56,40},{64,... | collective-permute-start | bytes 393224 | tf_op jit(solution)/shard_map/ppermute | solution.py:76
  144.6 5.9 %collective-permute-done.7 = bf16[4,8,2048]{2,1,0:T(8,128)(2,1)S(1)} collective-permute-done((bf16[4,8,2048]{2,1,0:T(8,128)(2,1)}, bf16[4,8,2048]{2,1,0:T(8,128)(2,1)S(1)}, u32[]{:S(2)}, u32[]{:S(2)}) %collective-permute-start.7) | collective-permute-done | bytes 131104 | tf_op jit(solution)/shard_map/ppermute | solution.py:76
  150.5 2.5 collective-permute-done.8
  153.1 1.7 fusion.7
  154.8 4.0 %all-to-all-start.3 = ((bf16[8,8,2048]{2,1,0:T(8,128)(2,1)}), bf16[8,8,2048]{2,1,0:T(8,128)(2,1)S(1)}, u32[]{:S(2)}, u32[]{:S(2)}) async-start(bf16[8,8,2048]{2,1,0:T(8,128)(2,1)} %fusion.7), calls=%async_computation.3 | async-start | bytes 524288 | tf_op jit(solution)/shard_map/all_to_all | solution.py:28
  158.8 45.4 %all-to-all-done.3 = bf16[8,8,2048]{2,1,0:T(8,128)(2,1)S(1)} async-done(((bf16[8,8,2048]{2,1,0:T(8,128)(2,1)}), bf16[8,8,2048]{2,1,0:T(8,128)(2,1)S(1)}, u32[]{:S(2)}, u32[]{:S(2)}) %all-to-all-start.3) | async-done | bytes 262176 | tf_op jit(solution)/shard_map/all_to_all | solution.py:28
  204.3 9.3 %all-gather.2.cloned.1.call-done = bf16[12288,256]{1,0:T(8,128)(2,1)} async-done(((bf16[384,256]{1,0:T(8,128)(2,1)}), bf16[12288,256]{1,0:T(8,128)(2,1)}) %all-gather.2.cloned.1.call-update) | async-done | bytes 6291472 | tf_op jit(solution)/shard_map/all_gather | solution.py:261
  213.7 2.5 slice.133
  216.6 1.6 collective-permute-start.13
  218.3 10.3 %all_to_all.41 = bf16[8,8,2048]{2,1,0:T(8,128)(2,1)} all-to-all(bf16[8,8,2048]{2,1,0:T(8,128)(2,1)S(1)} %broadcast_in_dim.57), channel_id=1, replica_groups=mesh['grp'=2,'fs'=32,'tp'=8] {'tp'}, dimensions={0} | all-to-all | bytes 524288 | tf_op jit(solution)/shard_map/all_to_all | solution.py:28
  228.6 4.2 %hidden_second.1 = bf16[64,512]{1,0:T(8,128)(2,1)} custom-call(bf16[64,2048]{1,0:T(8,128)(2,1)} %bitcast.114, bf16[32,384,256]{2,1,0:T(8,128)(2,1)} %bitcast.98), custom_call_target="tpu_custom_call" | custom-call | tf_op jit(solution)/shard_map/hidden_second/pallas_call | solution.py:193
  233.7 13.5 %all_to_all.42.h_ref = bf16[8,64,512]{2,1,0:T(8,128)(2,1)} all-to-all(bf16[8,64,512]{2,1,0:T(8,128)(2,1)S(1)} %broadcast_in_dim.58), channel_id=1, replica_groups=mesh['grp'=2,'fs'=32,'tp'=8] {'tp'}, dimensions={0} | all-to-all | bytes 1048576 | tf_op jit(solution)/shard_map/all_to_all | solution.py:28
  247.2 3.6 down_second.1
  250.8 6.5 %all-to-all-start.6 = ((f32[8,8,256]{2,1,0:T(8,128)}), f32[8,8,256]{2,1,0:T(8,128)S(1)}, u32[]{:S(2)}, u32[]{:S(2)}) async-start(f32[8,8,256]{2,1,0:T(8,128)} %bitcast.119), calls=%async_computation.6 | async-start | bytes 131072 | tf_op jit(solution)/shard_map/all_to_all | solution.py:28
  257.3 3.1 all-to-all-done.6
  260.4 1.7 broadcast_select_fusion
  262.2 1.7 collective-permute-start.14
  263.8 1.6 collective-permute-start.15
  266.2 17.2 %all-to-all-start.7 = ((bf16[8,8,2048]{2,1,0:T(8,128)(2,1)}), bf16[8,8,2048]{2,1,0:T(8,128)(2,1)S(1)}, u32[]{:S(2)}, u32[]{:S(2)}) async-start(bf16[8,8,2048]{2,1,0:T(8,128)(2,1)} %broadcast_in_dim.59), calls=%async_computation.7 | async-start | bytes 524288 | tf_op jit(solution)/shard_map/all_to_all | solution.py:28
  285.7 1.4 select_select_fusion
  287.1 1.0 slice_bitcast_fusion
  288.1 1.3 collective-permute-start.16
  289.4 1.3 collective-permute-start.17
  290.8 24.1 %all-to-all-done.7 = bf16[8,8,2048]{2,1,0:T(8,128)(2,1)S(1)} async-done(((bf16[8,8,2048]{2,1,0:T(8,128)(2,1)}), bf16[8,8,2048]{2,1,0:T(8,128)(2,1)S(1)}, u32[]{:S(2)}, u32[]{:S(2)}) %all-to-all-start.7) | async-done | bytes 262176 | tf_op jit(solution)/shard_map/all_to_all | solution.py:28
  314.9 13.2 %collective-permute-start.10 = (bf16[4,8,2048]{2,1,0:T(8,128)(2,1)S(1)}, bf16[4,8,2048]{2,1,0:T(8,128)(2,1)S(1)}, u32[]{:S(2)}, u32[]{:S(2)}) collective-permute-start(bf16[4,8,2048]{2,1,0:T(8,128)(2,1)S(1)} %get-tuple-element.41), channel_id=1, source_target_pairs={{0,16},{8,24},{16,32},{24,40},{32,48},{40,56},{48,64},{56,72},{64,... | collective-permute-start | bytes 393224 | tf_op jit(solution)/shard_map/ppermute | solution.py:76
  328.1 2.0 collective-permute-start.11
  330.1 2.2 collective-permute-start.9
  332.4 10.3 %collective-permute-done.9 = bf16[8,8,2048]{2,1,0:T(8,128)(2,1)S(1)} collective-permute-done((bf16[8,8,2048]{2,1,0:T(8,128)(2,1)S(1)}, bf16[8,8,2048]{2,1,0:T(8,128)(2,1)S(1)}, u32[]{:S(2)}, u32[]{:S(2)}) %collective-permute-start.9) | collective-permute-done | bytes 262176 | tf_op jit(solution)/shard_map/ppermute | solution.py:76
  342.8 1.9 collective-permute-start.12
  344.8 8.0 %collective-permute-done.12 = bf16[8,8,2048]{2,1,0:T(8,128)(2,1)S(1)} collective-permute-done((bf16[8,8,2048]{2,1,0:T(8,128)(2,1)S(1)}, bf16[8,8,2048]{2,1,0:T(8,128)(2,1)S(1)}, u32[]{:S(2)}, u32[]{:S(2)}) %collective-permute-start.12) | collective-permute-done | bytes 262176 | tf_op jit(solution)/shard_map/ppermute | solution.py:76
  352.9 1.2 broadcast_select_fusion.1
  (85 shorter events, 14.7 us)
Async XLA Ops:
  7.2 9.4 %copy-start.7 = (f32[128,256]{1,0:T(8,128)S(1)}, f32[128,256]{1,0:T(8,128)}, u32[]{:S(2)}) copy-start(f32[128,256]{1,0:T(8,128)} %param.13) | copy-start | bytes 393220
  7.2 206.5 %all-gather.2.cloned.1.call-start = ((), (), s32[]{:S(2)}) async-start(), calls=%async_computation.8 | async-start | bytes 6488064 | tf_op jit(solution)/shard_map/all_gather | solution.py:261
  9.3 0.7 copy-start.6
  11.8 8.2 %all-to-all-start = ((bf16[8,2,8,512]{3,2,1,0:T(8,128)(2,1)}), bf16[8,2,8,512]{3,2,1,0:T(8,128)(2,1)S(1)}, u32[]{:S(2)}, u32[]{:S(2)}) async-start(bf16[8,2,8,512]{3,2,1,0:T(8,128)(2,1)} %maximum_bitcast_fusion.1), calls=%async_computation | async-start | bytes 262144 | tf_op jit(solution)/shard_map/all_to_all | solution.py:28
  20.7 57.2 %collective-permute-start = (bf16[512,128]{1,0:T(8,128)(2,1)S(1)}, bf16[512,128]{1,0:T(8,128)(2,1)S(1)}, u32[]{:S(2)}, u32[]{:S(2)}) collective-permute-start(bf16[512,128]{1,0:T(8,128)(2,1)S(1)} %pad_maximum_fusion.3), channel_id=1, source_target_pairs={{0,6},{1,7},{2,0},{3,1},{4,2},{5,3},{6,4},{7,5},{8,14},{9,15},{10,... | collective-permute-start | bytes 393224 | tf_op jit(solution)/shard_map/ppermute | solution.py:57
  24.6 53.4 %collective-permute-start.1 = (bf16[512,128]{1,0:T(8,128)(2,1)S(1)}, bf16[512,128]{1,0:T(8,128)(2,1)S(1)}, u32[]{:S(2)}, u32[]{:S(2)}) collective-permute-start(bf16[512,128]{1,0:T(8,128)(2,1)S(1)} %pad_maximum_fusion.3), channel_id=1, source_target_pairs={{0,4},{1,5},{2,6},{3,7},{4,0},{5,1},{6,2},{7,3},{8,12},{9,13},{10,... | collective-permute-start | bytes 393224 | tf_op jit(solution)/shard_map/ppermute | solution.py:57
  28.6 49.4 %collective-permute-start.2 = (bf16[512,128]{1,0:T(8,128)(2,1)S(1)}, bf16[512,128]{1,0:T(8,128)(2,1)S(1)}, u32[]{:S(2)}, u32[]{:S(2)}) collective-permute-start(bf16[512,128]{1,0:T(8,128)(2,1)S(1)} %pad_maximum_fusion.3), channel_id=1, source_target_pairs={{0,2},{1,3},{2,4},{3,5},{4,6},{5,7},{6,0},{7,1},{8,10},{9,11},{10,... | collective-permute-start | bytes 393224 | tf_op jit(solution)/shard_map/ppermute | solution.py:57
  32.0 77.9 %all-to-all-start.1 = ((bf16[32,2,8,128]{3,2,1,0:T(8,128)(2,1)}), bf16[32,2,8,128]{3,2,1,0:T(8,128)(2,1)S(1)}, u32[]{:S(2)}, u32[]{:S(2)}) async-start(bf16[32,2,8,128]{3,2,1,0:T(8,128)(2,1)} %bitcast.3), calls=%async_computation.1 | async-start | bytes 262144 | tf_op jit(solution)/shard_map/all_to_all | solution.py:28
  78.0 3.8 %collective-permute-start.3 = (bf16[4,512,128]{2,1,0:T(8,128)(2,1)S(1)}, bf16[4,512,128]{2,1,0:T(8,128)(2,1)S(1)}, u32[]{:S(2)}, u32[]{:S(2)}) collective-permute-start(bf16[4,512,128]{2,1,0:T(8,128)(2,1)S(1)} %bitcast_dynamic-update-slice_fusion.3), channel_id=1, source_target_pairs={{0,1},{1,0},{2,3},{3,2},{4,5},{5,4},{6,7},{7,6},{8,9},{9,8},{10,11... | collective-permute-start | bytes 1572872 | tf_op jit(solution)/shard_map/ppermute | solution.py:68
  82.0 40.0 %copy-start = (bf16[256,2048]{1,0:T(8,128)(2,1)S(1)}, bf16[256,2048]{1,0:T(8,128)(2,1)}, u32[]{:S(2)}) copy-start(bf16[256,2048]{1,0:T(8,128)(2,1)} %param.9) | copy-start | bytes 3145732
  120.0 4.0 %collective-permute-start.4 = (bf16[4,512,128]{2,1,0:T(8,128)(2,1)S(1)}, bf16[4,512,128]{2,1,0:T(8,128)(2,1)}, u32[]{:S(2)}, u32[]{:S(2)}) collective-permute-start(bf16[4,512,128]{2,1,0:T(8,128)(2,1)S(1)} %all_to_all.40), channel_id=1, source_target_pairs={{0,1},{1,0},{2,3},{3,2},{4,5},{5,4},{6,7},{7,6},{8,9},{9,8},{10,11... | collective-permute-start | bytes 1572872 | tf_op jit(solution)/shard_map/ppermute | solution.py:49
  125.7 0.8 copy-start.5
  125.9 1.5 copy-start.2
  128.1 24.9 %collective-permute-start.5 = (bf16[8,8,2048]{2,1,0:T(8,128)(2,1)}, bf16[8,8,2048]{2,1,0:T(8,128)(2,1)S(1)}, u32[]{:S(2)}, u32[]{:S(2)}) collective-permute-start(bf16[8,8,2048]{2,1,0:T(8,128)(2,1)} %get-tuple-element.34), channel_id=1, source_target_pairs={{0,8},{8,16},{16,24},{24,32},{32,40},{40,48},{48,56},{56,64},{64,7... | collective-permute-start | bytes 786440 | tf_op jit(solution)/shard_map/ppermute | solution.py:76
  130.2 22.9 %collective-permute-start.6 = (bf16[8,8,2048]{2,1,0:T(8,128)(2,1)S(1)}, bf16[8,8,2048]{2,1,0:T(8,128)(2,1)S(1)}, u32[]{:S(2)}, u32[]{:S(2)}) collective-permute-start(bf16[8,8,2048]{2,1,0:T(8,128)(2,1)S(1)} %get-tuple-element.33), channel_id=1, source_target_pairs={{0,248},{8,0},{16,8},{24,16},{32,24},{40,32},{48,40},{56,48},{64,5... | collective-permute-start | bytes 786440 | tf_op jit(solution)/shard_map/ppermute | solution.py:76
  135.9 14.6 %collective-permute-start.7 = (bf16[4,8,2048]{2,1,0:T(8,128)(2,1)}, bf16[4,8,2048]{2,1,0:T(8,128)(2,1)S(1)}, u32[]{:S(2)}, u32[]{:S(2)}) collective-permute-start(bf16[4,8,2048]{2,1,0:T(8,128)(2,1)} %slice_bitcast_fusion.2), channel_id=1, source_target_pairs={{0,16},{8,24},{16,32},{24,40},{32,48},{40,56},{48,64},{56,72},{64,... | collective-permute-start | bytes 393224 | tf_op jit(solution)/shard_map/ppermute | solution.py:76
  138.5 14.5 %collective-permute-start.8 = (bf16[4,8,2048]{2,1,0:T(8,128)(2,1)}, bf16[4,8,2048]{2,1,0:T(8,128)(2,1)}, u32[]{:S(2)}, u32[]{:S(2)}) collective-permute-start(bf16[4,8,2048]{2,1,0:T(8,128)(2,1)} %dynamic-slice_bitcast_fusion.3), channel_id=1, source_target_pairs={{0,240},{8,248},{16,0},{24,8},{32,16},{40,24},{48,32},{56,40},{64,... | collective-permute-start | bytes 393224 | tf_op jit(solution)/shard_map/ppermute | solution.py:76
  154.8 49.3 %all-to-all-start.3 = ((bf16[8,8,2048]{2,1,0:T(8,128)(2,1)}), bf16[8,8,2048]{2,1,0:T(8,128)(2,1)S(1)}, u32[]{:S(2)}, u32[]{:S(2)}) async-start(bf16[8,8,2048]{2,1,0:T(8,128)(2,1)} %fusion.7), calls=%async_computation.3 | async-start | bytes 524288 | tf_op jit(solution)/shard_map/all_to_all | solution.py:28
  216.6 16.2 %copy-start.1 = (bf16[2,32,64,128]{3,2,1,0:T(8,128)(2,1)}, bf16[2,32,64,128]{3,2,1,0:T(8,128)(2,1)S(1)}, u32[]{:S(2)}) copy-start(bf16[2,32,64,128]{3,2,1,0:T(8,128)(2,1)S(1)} %copy.40) | copy-start | bytes 3145732
  216.6 43.8 %collective-permute-start.13 = (bf16[2,2048,128]{2,1,0:T(8,128)(2,1)S(1)}, bf16[2,2048,128]{2,1,0:T(8,128)(2,1)}, u32[]{:S(2)}, u32[]{:S(2)}) collective-permute-start(bf16[2,2048,128]{2,1,0:T(8,128)(2,1)S(1)} %bitcast.107), channel_id=1, source_target_pairs={{0,1},{8,9},{16,17},{24,25},{33,32},{41,40},{49,48},{57,56},{66,67... | collective-permute-start | bytes 3145736 | tf_op jit(solution)/shard_map/ppermute | solution.py:136
  250.8 9.6 %all-to-all-start.6 = ((f32[8,8,256]{2,1,0:T(8,128)}), f32[8,8,256]{2,1,0:T(8,128)S(1)}, u32[]{:S(2)}, u32[]{:S(2)}) async-start(f32[8,8,256]{2,1,0:T(8,128)} %bitcast.119), calls=%async_computation.6 | async-start | bytes 131072 | tf_op jit(solution)/shard_map/all_to_all | solution.py:28
  260.4 24.0 %copy-start.3 = (bf16[8,256,128]{2,1,0:T(8,128)(2,1)S(1)}, bf16[8,256,128]{2,1,0:T(8,128)(2,1)}, u32[]{:S(2)}) copy-start(bf16[8,256,128]{2,1,0:T(8,128)(2,1)} %get-tuple-element.26) | copy-start | bytes 1572868
  262.2 23.6 %collective-permute-start.14 = (bf16[2,2048,128]{2,1,0:T(8,128)(2,1)S(1)}, bf16[2,2048,128]{2,1,0:T(8,128)(2,1)}, u32[]{:S(2)}, u32[]{:S(2)}) collective-permute-start(bf16[2,2048,128]{2,1,0:T(8,128)(2,1)S(1)} %broadcast_select_fusion), channel_id=1, source_target_pairs={{0,2},{1,3},{8,10},{9,11},{16,18},{17,19},{24,26},{25,27},{32,34},... | collective-permute-start | bytes 3145736 | tf_op jit(solution)/shard_map/ppermute | solution.py:136
  263.8 21.9 %collective-permute-start.15 = (bf16[2,2048,128]{2,1,0:T(8,128)(2,1)S(1)}, bf16[2,2048,128]{2,1,0:T(8,128)(2,1)}, u32[]{:S(2)}, u32[]{:S(2)}) collective-permute-start(bf16[2,2048,128]{2,1,0:T(8,128)(2,1)S(1)} %broadcast_select_fusion), channel_id=1, source_target_pairs={{0,6},{1,7},{8,14},{9,15},{16,22},{17,23},{24,30},{25,31},{32,38},... | collective-permute-start | bytes 3145736 | tf_op jit(solution)/shard_map/ppermute | solution.py:136
  266.2 48.7 %all-to-all-start.7 = ((bf16[8,8,2048]{2,1,0:T(8,128)(2,1)}), bf16[8,8,2048]{2,1,0:T(8,128)(2,1)S(1)}, u32[]{:S(2)}, u32[]{:S(2)}) async-start(bf16[8,8,2048]{2,1,0:T(8,128)(2,1)} %broadcast_in_dim.59), calls=%async_computation.7 | async-start | bytes 524288 | tf_op jit(solution)/shard_map/all_to_all | solution.py:28
  288.1 64.7 %collective-permute-start.16 = (bf16[2048,128]{1,0:T(8,128)(2,1)}, bf16[2048,128]{1,0:T(8,128)(2,1)S(1)}, u32[]{:S(2)}, u32[]{:S(2)}) collective-permute-start(bf16[2048,128]{1,0:T(8,128)(2,1)} %get-tuple-element.31), channel_id=1, source_target_pairs={{2,4},{3,5},{10,12},{11,13},{18,20},{19,21},{26,28},{27,29},{34,36... | collective-permute-start | bytes 1572872 | tf_op jit(solution)/shard_map/ppermute | solution.py:136
  289.4 63.5 %collective-permute-start.17 = (bf16[2048,128]{1,0:T(8,128)(2,1)}, bf16[2048,128]{1,0:T(8,128)(2,1)S(1)}, u32[]{:S(2)}, u32[]{:S(2)}) collective-permute-start(bf16[2048,128]{1,0:T(8,128)(2,1)} %get-tuple-element.30), channel_id=1, source_target_pairs={{6,4},{7,5},{14,12},{15,13},{22,20},{23,21},{30,28},{31,29},{38,36... | collective-permute-start | bytes 1572872 | tf_op jit(solution)/shard_map/ppermute | solution.py:136
  314.9 29.9 %collective-permute-start.10 = (bf16[4,8,2048]{2,1,0:T(8,128)(2,1)S(1)}, bf16[4,8,2048]{2,1,0:T(8,128)(2,1)S(1)}, u32[]{:S(2)}, u32[]{:S(2)}) collective-permute-start(bf16[4,8,2048]{2,1,0:T(8,128)(2,1)S(1)} %get-tuple-element.41), channel_id=1, source_target_pairs={{0,16},{8,24},{16,32},{24,40},{32,48},{40,56},{48,64},{56,72},{64,... | collective-permute-start | bytes 393224 | tf_op jit(solution)/shard_map/ppermute | solution.py:76
  328.1 16.7 %collective-permute-start.11 = (bf16[4,8,2048]{2,1,0:T(8,128)(2,1)S(1)}, bf16[4,8,2048]{2,1,0:T(8,128)(2,1)S(1)}, u32[]{:S(2)}, u32[]{:S(2)}) collective-permute-start(bf16[4,8,2048]{2,1,0:T(8,128)(2,1)S(1)} %get-tuple-element.42), channel_id=1, source_target_pairs={{0,240},{8,248},{16,0},{24,8},{32,16},{40,24},{48,32},{56,40},{64,... | collective-permute-start | bytes 393224 | tf_op jit(solution)/shard_map/ppermute | solution.py:76
  330.1 12.7 %collective-permute-start.9 = (bf16[8,8,2048]{2,1,0:T(8,128)(2,1)S(1)}, bf16[8,8,2048]{2,1,0:T(8,128)(2,1)S(1)}, u32[]{:S(2)}, u32[]{:S(2)}) collective-permute-start(bf16[8,8,2048]{2,1,0:T(8,128)(2,1)S(1)} %all-to-all-done.7), channel_id=1, source_target_pairs={{0,248},{8,0},{16,8},{24,16},{32,24},{40,32},{48,40},{56,48},{64,5... | collective-permute-start | bytes 786440 | tf_op jit(solution)/shard_map/ppermute | solution.py:76
  342.8 10.1 %collective-permute-start.12 = (bf16[8,8,2048]{2,1,0:T(8,128)(2,1)S(1)}, bf16[8,8,2048]{2,1,0:T(8,128)(2,1)S(1)}, u32[]{:S(2)}, u32[]{:S(2)}) collective-permute-start(bf16[8,8,2048]{2,1,0:T(8,128)(2,1)S(1)} %all-to-all-done.7), channel_id=1, source_target_pairs={{0,8},{8,16},{16,24},{24,32},{32,40},{40,48},{48,56},{56,64},{64,7... | collective-permute-start | bytes 786440 | tf_op jit(solution)/shard_map/ppermute | solution.py:76
  352.9 1.3 copy-start.4
Sparse Core Ops, SparseCore 0:
  10.7 202.9 all-gather.1
where the time goes:
time: 363 us; the launch traced here: 361 us
  waiting for transfers between devices  142 us (39%)
  starting transfers between devices  135 us (37%)
  blocking collectives  33.8 us (9%)
  between operations  14.8 us (4%)
  other arithmetic  12.8 us (4%)
  local copies, waits for them, and re-layouts  12.7 us (3%)
  Pallas kernels  7.79 us (2%)
    all_to_all x5, waiting for transfers between devices, exchange(): lax.all_to_all(blocks, axis, split_axis=0, concat_axis=0, tiled=True, axi...  104 us
    all_to_all x5, starting transfers between devices, exchange(): lax.all_to_all(blocks, axis, split_axis=0, concat_axis=0, tiled=True, axi...  78.3 us
    ppermute x8, starting transfers between devices, shift(): return lax.ppermute(array, 'fs', [(i, (i + steps) % n) for i in range(n)])  34.4 us
    all_to_all x3, blocking collectives, exchange(): lax.all_to_all(blocks, axis, split_axis=0, concat_axis=0, tiled=True, axi...  33.8 us
    ppermute x8, waiting for transfers between devices, shift(): return lax.ppermute(array, 'fs', [(i, (i + steps) % n) for i in range(n)])  26.8 us
    ppermute x3, starting transfers between devices, shift_tp(): return lax.ppermute(array, 'tp', [(i, (i + steps) % n) for i in range(n)])  11.2 us
    all_gather x1, waiting for transfers between devices, on_device(): lax.all_gather(row_major(jnp.concatenate(pack, axis=0)), 'fs', axis=0, ti...  9.33 us
    ppermute x5, starting transfers between devices, hop(): lax.ppermute(array, ('fs', 'tp'), [pair for f in range(n) for pair in pai...  7.55 us
  transfers between devices with their start and end apart: 24, of which 12 were waited for; matrix products, arithmetic and copies ran while one was open for 5% of the time, Pallas kernels for 2%

commit v1 on v0

--- a/solution.py
+++ b/solution.py
@@ -136,10 +136,10 @@
         return lax.ppermute(array, ("fs", "tp"), [pair for f in range(n) for pair in pairs(f)])
 
     def first():
-        both = whole[:, : 4 * rows].reshape(planes, 2, 2, rows, cols)
-        both = jnp.where(me % per // 2 == 0, both[:, :, 0], both[:, :, 1])
-        both = jnp.where(me % 2 == 0, both[..., :lanes], both[..., lanes:])
-        return both.transpose(1, 0, 2, 3).reshape(2, planes * rows, lanes)
+        half = me % per // 2 * rows
+        both = [lax.dynamic_slice(whole, (0, 2 * m * rows + half, 0), (planes, rows, cols)) for m in range(2)]
+        both = [jnp.where(me % 2 == 0, w[..., :lanes], w[..., lanes:]) for w in both]
+        return jnp.stack([w.reshape(planes * rows, lanes) for w in both])
 
     def second(array):
         other = hop(array, lambda f: [(f * n_tp + f // per, f * n_tp + (f // per ^ 1))])

time: 363 us -> 359 us (0.989)
  the two profiles are of different devices: /device:TPU:44 before, /device:TPU:36 now
where the time goes in v1:
time: 359 us; the launch traced here: 358 us
  starting transfers between devices  137 us (38%)
  waiting for transfers between devices  134 us (37%)
  blocking collectives  33.5 us (9%)
  other arithmetic  16.6 us (5%)
  between operations  14.8 us (4%)
  local copies, waits for them, and re-layouts  12.7 us (4%)
  Pallas kernels  7.78 us (2%)
    all_to_all x5, waiting for transfers between devices, exchange(): lax.all_to_all(blocks, axis, split_axis=0, concat_axis=0, tiled=True, axi...  100 us
    all_to_all x5, starting transfers between devices, exchange(): lax.all_to_all(blocks, axis, split_axis=0, concat_axis=0, tiled=True, axi...  79.3 us
    ppermute x8, starting transfers between devices, shift(): return lax.ppermute(array, 'fs', [(i, (i + steps) % n) for i in range(n)])  36.1 us
    all_to_all x3, blocking collectives, exchange(): lax.all_to_all(blocks, axis, split_axis=0, concat_axis=0, tiled=True, axi...  33.5 us
    ppermute x8, waiting for transfers between devices, shift(): return lax.ppermute(array, 'fs', [(i, (i + steps) % n) for i in range(n)])  22.4 us
    ppermute x3, starting transfers between devices, shift_tp(): return lax.ppermute(array, 'tp', [(i, (i + steps) % n) for i in range(n)])  11.1 us
    all_gather x1, waiting for transfers between devices, on_device(): lax.all_gather(row_major(jnp.concatenate(pack, axis=0)), 'fs', axis=0, ti...  9.22 us
  transfers between devices with their start and end apart: 24, of which 11 were waited for; matrix products, arithmetic and copies ran while one was open for 6% of the time, Pallas kernels for 2%

profile of v1, /device:TPU:36, one launch (start us, length us, event | category | flops | bytes accessed | tf_op | source)
XLA Modules:
  0.0 357.6 jit_solution(10323218679501972134)
XLA Ops:
  7.3 1.1 multiply_convert_fusion
  10.0 1.1 fusion.16
  11.8 43.6 %all-to-all-start = ((bf16[8,2,8,512]{3,2,1,0:T(8,128)(2,1)}), bf16[8,2,8,512]{3,2,1,0:T(8,128)(2,1)S(1)}, u32[]{:S(2)}, u32[]{:S(2)}) async-start(bf16[8,2,8,512]{3,2,1,0:T(8,128)(2,1)} %maximum_bitcast_fusion.1), calls=%async_computation | async-start | bytes 262144 | tf_op jit(solution)/shard_map/all_to_all | solution.py:28
  55.4 3.4 all-to-all-done
  59.6 3.8 %collective-permute-start = (bf16[512,128]{1,0:T(8,128)(2,1)S(1)}, bf16[512,128]{1,0:T(8,128)(2,1)S(1)}, u32[]{:S(2)}, u32[]{:S(2)}) collective-permute-start(bf16[512,128]{1,0:T(8,128)(2,1)S(1)} %pad_maximum_fusion.4), channel_id=1, source_target_pairs={{0,6},{1,7},{2,0},{3,1},{4,2},{5,3},{6,4},{7,5},{8,14},{9,15},{10,... | collective-permute-start | bytes 393224 | tf_op jit(solution)/shard_map/ppermute | solution.py:57
  63.4 3.9 %collective-permute-start.1 = (bf16[512,128]{1,0:T(8,128)(2,1)S(1)}, bf16[512,128]{1,0:T(8,128)(2,1)S(1)}, u32[]{:S(2)}, u32[]{:S(2)}) collective-permute-start(bf16[512,128]{1,0:T(8,128)(2,1)S(1)} %pad_maximum_fusion.4), channel_id=1, source_target_pairs={{0,4},{1,5},{2,6},{3,7},{4,0},{5,1},{6,2},{7,3},{8,12},{9,13},{10,... | collective-permute-start | bytes 393224 | tf_op jit(solution)/shard_map/ppermute | solution.py:57
  67.4 3.4 collective-permute-start.2
  70.8 7.0 %all-to-all-start.1 = ((bf16[32,2,8,128]{3,2,1,0:T(8,128)(2,1)}), bf16[32,2,8,128]{3,2,1,0:T(8,128)(2,1)S(1)}, u32[]{:S(2)}, u32[]{:S(2)}) async-start(bf16[32,2,8,128]{3,2,1,0:T(8,128)(2,1)} %bitcast.3), calls=%async_computation.1 | async-start | bytes 262144 | tf_op jit(solution)/shard_map/all_to_all | solution.py:28
  78.0 2.0 collective-permute-start.3
  80.0 1.9 collective-permute-done.3
  82.1 27.6 %all-to-all-done.1 = bf16[32,2,8,128]{3,2,1,0:T(8,128)(2,1)S(1)} async-done(((bf16[32,2,8,128]{3,2,1,0:T(8,128)(2,1)}), bf16[32,2,8,128]{3,2,1,0:T(8,128)(2,1)S(1)}, u32[]{:S(2)}, u32[]{:S(2)}) %all-to-all-start.1) | async-done | bytes 131104 | tf_op jit(solution)/shard_map/all_to_all | solution.py:28
  109.7 10.0 %all_to_all.40 = bf16[4,512,128]{2,1,0:T(8,128)(2,1)S(1)} all-to-all(bf16[4,512,128]{2,1,0:T(8,128)(2,1)S(1)} %broadcast_in_dim.56), channel_id=1, replica_groups={{0,2,4,6},{1,3,5,7},{8,10,12,14},{9,11,13,15},{16,18,20,22},{17,19,21,2..., dimensions={0} | all-to-all | bytes 1048576 | tf_op jit(solution)/shard_map/all_to_all | solution.py:28
  119.8 1.9 collective-permute-start.4
  123.1 1.3 copy.32
  124.5 1.1 select_bitcast_fusion.1
  128.8 1.9 collective-permute-start.6
  130.7 4.0 %collective-permute-start.5 = (bf16[8,8,2048]{2,1,0:T(8,128)(2,1)S(1)}, bf16[8,8,2048]{2,1,0:T(8,128)(2,1)S(1)}, u32[]{:S(2)}, u32[]{:S(2)}) collective-permute-start(bf16[8,8,2048]{2,1,0:T(8,128)(2,1)S(1)} %get-tuple-element.36), channel_id=1, source_target_pairs={{0,8},{8,16},{16,24},{24,32},{32,40},{40,48},{48,56},{56,64},{64,7... | collective-permute-start | bytes 786440 | tf_op jit(solution)/shard_map/ppermute | solution.py:76
  135.3 2.4 collective-permute-start.8
  138.4 4.4 %collective-permute-start.7 = (bf16[4,8,2048]{2,1,0:T(8,128)(2,1)}, bf16[4,8,2048]{2,1,0:T(8,128)(2,1)}, u32[]{:S(2)}, u32[]{:S(2)}) collective-permute-start(bf16[4,8,2048]{2,1,0:T(8,128)(2,1)} %slice_bitcast_fusion.2), channel_id=1, source_target_pairs={{0,16},{8,24},{16,32},{24,40},{32,48},{40,56},{48,64},{56,72},{64,... | collective-permute-start | bytes 393224 | tf_op jit(solution)/shard_map/ppermute | solution.py:76
  142.8 9.3 %collective-permute-done.8 = bf16[4,8,2048]{2,1,0:T(8,128)(2,1)S(1)} collective-permute-done((bf16[4,8,2048]{2,1,0:T(8,128)(2,1)}, bf16[4,8,2048]{2,1,0:T(8,128)(2,1)S(1)}, u32[]{:S(2)}, u32[]{:S(2)}) %collective-permute-start.8) | collective-permute-done | bytes 131104 | tf_op jit(solution)/shard_map/ppermute | solution.py:76
  152.1 2.9 collective-permute-done.7
  155.0 1.7 fusion.5
  156.8 5.8 %all-to-all-start.3 = ((bf16[8,8,2048]{2,1,0:T(8,128)(2,1)}), bf16[8,8,2048]{2,1,0:T(8,128)(2,1)S(1)}, u32[]{:S(2)}, u32[]{:S(2)}) async-start(bf16[8,8,2048]{2,1,0:T(8,128)(2,1)} %fusion.5), calls=%async_computation.3 | async-start | bytes 524288 | tf_op jit(solution)/shard_map/all_to_all | solution.py:28
  162.5 43.2 %all-to-all-done.3 = bf16[8,8,2048]{2,1,0:T(8,128)(2,1)S(1)} async-done(((bf16[8,8,2048]{2,1,0:T(8,128)(2,1)}), bf16[8,8,2048]{2,1,0:T(8,128)(2,1)S(1)}, u32[]{:S(2)}, u32[]{:S(2)}) %all-to-all-start.3) | async-done | bytes 262176 | tf_op jit(solution)/shard_map/all_to_all | solution.py:28
  205.9 9.2 %all-gather.2.cloned.1.call-done = bf16[12288,256]{1,0:T(8,128)(2,1)} async-done(((bf16[384,256]{1,0:T(8,128)(2,1)}), bf16[12288,256]{1,0:T(8,128)(2,1)}) %all-gather.2.cloned.1.call-update) | async-done | bytes 6291472 | tf_op jit(solution)/shard_map/all_gather | solution.py:261
  215.1 1.9 dynamic-slice_select_fusion.1
  219.7 9.9 %all_to_all.41 = bf16[8,8,2048]{2,1,0:T(8,128)(2,1)} all-to-all(bf16[8,8,2048]{2,1,0:T(8,128)(2,1)S(1)} %broadcast_in_dim.57), channel_id=1, replica_groups=mesh['grp'=2,'fs'=32,'tp'=8] {'tp'}, dimensions={0} | all-to-all | bytes 524288 | tf_op jit(solution)/shard_map/all_to_all | solution.py:28
  229.6 4.2 %hidden_second.1 = bf16[64,512]{1,0:T(8,128)(2,1)} custom-call(bf16[64,2048]{1,0:T(8,128)(2,1)} %bitcast.113, bf16[32,384,256]{2,1,0:T(8,128)(2,1)} %bitcast.93), custom_call_target="tpu_custom_call" | custom-call | tf_op jit(solution)/shard_map/hidden_second/pallas_call | solution.py:193
  234.7 13.5 %all_to_all.42.h_ref = bf16[8,64,512]{2,1,0:T(8,128)(2,1)} all-to-all(bf16[8,64,512]{2,1,0:T(8,128)(2,1)S(1)} %broadcast_in_dim.58), channel_id=1, replica_groups=mesh['grp'=2,'fs'=32,'tp'=8] {'tp'}, dimensions={0} | all-to-all | bytes 1048576 | tf_op jit(solution)/shard_map/all_to_all | solution.py:28
  248.2 3.6 down_second.1
  251.8 6.5 %all-to-all-start.6 = ((f32[8,8,256]{2,1,0:T(8,128)}), f32[8,8,256]{2,1,0:T(8,128)S(1)}, u32[]{:S(2)}, u32[]{:S(2)}) async-start(f32[8,8,256]{2,1,0:T(8,128)} %bitcast.118), calls=%async_computation.6 | async-start | bytes 131072 | tf_op jit(solution)/shard_map/all_to_all | solution.py:28
  258.3 3.1 all-to-all-done.6
  261.4 1.2 broadcast_select_fusion
  262.7 1.6 collective-permute-start.14
  264.3 1.6 collective-permute-start.15
  267.5 16.5 %all-to-all-start.7 = ((bf16[8,8,2048]{2,1,0:T(8,128)(2,1)}), bf16[8,8,2048]{2,1,0:T(8,128)(2,1)S(1)}, u32[]{:S(2)}, u32[]{:S(2)}) async-start(bf16[8,8,2048]{2,1,0:T(8,128)(2,1)} %broadcast_in_dim.59), calls=%async_computation.7 | async-start | bytes 524288 | tf_op jit(solution)/shard_map/all_to_all | solution.py:28
  285.0 1.4 copy.38
  287.4 1.4 select_select_fusion
  289.9 1.3 collective-permute-start.17
  291.2 1.3 collective-permute-start.16
  292.5 23.1 %all-to-all-done.7 = bf16[8,8,2048]{2,1,0:T(8,128)(2,1)S(1)} async-done(((bf16[8,8,2048]{2,1,0:T(8,128)(2,1)}), bf16[8,8,2048]{2,1,0:T(8,128)(2,1)S(1)}, u32[]{:S(2)}, u32[]{:S(2)}) %all-to-all-start.7) | async-done | bytes 262176 | tf_op jit(solution)/shard_map/all_to_all | solution.py:28
  315.6 13.1 %collective-permute-start.11 = (bf16[4,8,2048]{2,1,0:T(8,128)(2,1)S(1)}, bf16[4,8,2048]{2,1,0:T(8,128)(2,1)S(1)}, u32[]{:S(2)}, u32[]{:S(2)}) collective-permute-start(bf16[4,8,2048]{2,1,0:T(8,128)(2,1)S(1)} %get-tuple-element.44), channel_id=1, source_target_pairs={{0,240},{8,248},{16,0},{24,8},{32,16},{40,24},{48,32},{56,40},{64,... | collective-permute-start | bytes 393224 | tf_op jit(solution)/shard_map/ppermute | solution.py:76
  328.6 2.0 collective-permute-start.10
  330.6 5.0 %collective-permute-start.9 = (bf16[8,8,2048]{2,1,0:T(8,128)(2,1)S(1)}, bf16[8,8,2048]{2,1,0:T(8,128)(2,1)S(1)}, u32[]{:S(2)}, u32[]{:S(2)}) collective-permute-start(bf16[8,8,2048]{2,1,0:T(8,128)(2,1)S(1)} %all-to-all-done.7), channel_id=1, source_target_pairs={{0,248},{8,0},{16,8},{24,16},{32,24},{40,32},{48,40},{56,48},{64,5... | collective-permute-start | bytes 786440 | tf_op jit(solution)/shard_map/ppermute | solution.py:76
  335.8 3.7 %collective-permute-done.9 = bf16[8,8,2048]{2,1,0:T(8,128)(2,1)S(1)} collective-permute-done((bf16[8,8,2048]{2,1,0:T(8,128)(2,1)S(1)}, bf16[8,8,2048]{2,1,0:T(8,128)(2,1)S(1)}, u32[]{:S(2)}, u32[]{:S(2)}) %collective-permute-start.9) | collective-permute-done | bytes 262176 | tf_op jit(solution)/shard_map/ppermute | solution.py:76
  339.5 3.4 collective-permute-start.12
  343.0 6.5 %collective-permute-done.12 = bf16[8,8,2048]{2,1,0:T(8,128)(2,1)S(1)} collective-permute-done((bf16[8,8,2048]{2,1,0:T(8,128)(2,1)S(1)}, bf16[8,8,2048]{2,1,0:T(8,128)(2,1)S(1)}, u32[]{:S(2)}, u32[]{:S(2)}) %collective-permute-start.12) | collective-permute-done | bytes 262176 | tf_op jit(solution)/shard_map/ppermute | solution.py:76
  349.5 1.3 broadcast_select_fusion.1
  (83 shorter events, 17.9 us)
Async XLA Ops:
  7.2 48.2 %copy-start.7 = (f32[128,256]{1,0:T(8,128)S(1)}, f32[128,256]{1,0:T(8,128)}, u32[]{:S(2)}) copy-start(f32[128,256]{1,0:T(8,128)} %param.13) | copy-start | bytes 393220
  7.2 207.9 %all-gather.2.cloned.1.call-start = ((), (), s32[]{:S(2)}) async-start(), calls=%async_computation.8 | async-start | bytes 6488064 | tf_op jit(solution)/shard_map/all_gather | solution.py:261
  9.3 0.7 copy-start.6
  11.8 47.0 %all-to-all-start = ((bf16[8,2,8,512]{3,2,1,0:T(8,128)(2,1)}), bf16[8,2,8,512]{3,2,1,0:T(8,128)(2,1)S(1)}, u32[]{:S(2)}, u32[]{:S(2)}) async-start(bf16[8,2,8,512]{3,2,1,0:T(8,128)(2,1)} %maximum_bitcast_fusion.1), calls=%async_computation | async-start | bytes 262144 | tf_op jit(solution)/shard_map/all_to_all | solution.py:28
  59.6 18.3 %collective-permute-start = (bf16[512,128]{1,0:T(8,128)(2,1)S(1)}, bf16[512,128]{1,0:T(8,128)(2,1)S(1)}, u32[]{:S(2)}, u32[]{:S(2)}) collective-permute-start(bf16[512,128]{1,0:T(8,128)(2,1)S(1)} %pad_maximum_fusion.4), channel_id=1, source_target_pairs={{0,6},{1,7},{2,0},{3,1},{4,2},{5,3},{6,4},{7,5},{8,14},{9,15},{10,... | collective-permute-start | bytes 393224 | tf_op jit(solution)/shard_map/ppermute | solution.py:57
  63.4 14.5 %collective-permute-start.1 = (bf16[512,128]{1,0:T(8,128)(2,1)S(1)}, bf16[512,128]{1,0:T(8,128)(2,1)S(1)}, u32[]{:S(2)}, u32[]{:S(2)}) collective-permute-start(bf16[512,128]{1,0:T(8,128)(2,1)S(1)} %pad_maximum_fusion.4), channel_id=1, source_target_pairs={{0,4},{1,5},{2,6},{3,7},{4,0},{5,1},{6,2},{7,3},{8,12},{9,13},{10,... | collective-permute-start | bytes 393224 | tf_op jit(solution)/shard_map/ppermute | solution.py:57
  67.4 10.6 %collective-permute-start.2 = (bf16[512,128]{1,0:T(8,128)(2,1)S(1)}, bf16[512,128]{1,0:T(8,128)(2,1)S(1)}, u32[]{:S(2)}, u32[]{:S(2)}) collective-permute-start(bf16[512,128]{1,0:T(8,128)(2,1)S(1)} %pad_maximum_fusion.4), channel_id=1, source_target_pairs={{0,2},{1,3},{2,4},{3,5},{4,6},{5,7},{6,0},{7,1},{8,10},{9,11},{10,... | collective-permute-start | bytes 393224 | tf_op jit(solution)/shard_map/ppermute | solution.py:57
  70.8 38.8 %all-to-all-start.1 = ((bf16[32,2,8,128]{3,2,1,0:T(8,128)(2,1)}), bf16[32,2,8,128]{3,2,1,0:T(8,128)(2,1)S(1)}, u32[]{:S(2)}, u32[]{:S(2)}) async-start(bf16[32,2,8,128]{3,2,1,0:T(8,128)(2,1)} %bitcast.3), calls=%async_computation.1 | async-start | bytes 262144 | tf_op jit(solution)/shard_map/all_to_all | solution.py:28
  78.0 3.8 %collective-permute-start.3 = (bf16[4,512,128]{2,1,0:T(8,128)(2,1)S(1)}, bf16[4,512,128]{2,1,0:T(8,128)(2,1)S(1)}, u32[]{:S(2)}, u32[]{:S(2)}) collective-permute-start(bf16[4,512,128]{2,1,0:T(8,128)(2,1)S(1)} %bitcast_dynamic-update-slice_fusion.3), channel_id=1, source_target_pairs={{0,1},{1,0},{2,3},{3,2},{4,5},{5,4},{6,7},{7,6},{8,9},{9,8},{10,11... | collective-permute-start | bytes 1572872 | tf_op jit(solution)/shard_map/ppermute | solution.py:68
  82.0 39.8 %copy-start = (bf16[256,2048]{1,0:T(8,128)(2,1)S(1)}, bf16[256,2048]{1,0:T(8,128)(2,1)}, u32[]{:S(2)}) copy-start(bf16[256,2048]{1,0:T(8,128)(2,1)} %param.9) | copy-start | bytes 3145732
  119.8 4.7 %collective-permute-start.4 = (bf16[4,512,128]{2,1,0:T(8,128)(2,1)S(1)}, bf16[4,512,128]{2,1,0:T(8,128)(2,1)}, u32[]{:S(2)}, u32[]{:S(2)}) collective-permute-start(bf16[4,512,128]{2,1,0:T(8,128)(2,1)S(1)} %all_to_all.40), channel_id=1, source_target_pairs={{0,1},{1,0},{2,3},{3,2},{4,5},{5,4},{6,7},{7,6},{8,9},{9,8},{10,11... | collective-permute-start | bytes 1572872 | tf_op jit(solution)/shard_map/ppermute | solution.py:49
  126.2 1.8 copy-start.3
  126.3 0.8 copy-start.5
  128.8 26.3 %collective-permute-start.6 = (bf16[8,8,2048]{2,1,0:T(8,128)(2,1)}, bf16[8,8,2048]{2,1,0:T(8,128)(2,1)S(1)}, u32[]{:S(2)}, u32[]{:S(2)}) collective-permute-start(bf16[8,8,2048]{2,1,0:T(8,128)(2,1)} %get-tuple-element.35), channel_id=1, source_target_pairs={{0,248},{8,0},{16,8},{24,16},{32,24},{40,32},{48,40},{56,48},{64,5... | collective-permute-start | bytes 786440 | tf_op jit(solution)/shard_map/ppermute | solution.py:76
  130.7 24.3 %collective-permute-start.5 = (bf16[8,8,2048]{2,1,0:T(8,128)(2,1)S(1)}, bf16[8,8,2048]{2,1,0:T(8,128)(2,1)S(1)}, u32[]{:S(2)}, u32[]{:S(2)}) collective-permute-start(bf16[8,8,2048]{2,1,0:T(8,128)(2,1)S(1)} %get-tuple-element.36), channel_id=1, source_target_pairs={{0,8},{8,16},{16,24},{24,32},{32,40},{40,48},{48,56},{56,64},{64,7... | collective-permute-start | bytes 786440 | tf_op jit(solution)/shard_map/ppermute | solution.py:76
  135.3 16.8 %collective-permute-start.8 = (bf16[4,8,2048]{2,1,0:T(8,128)(2,1)}, bf16[4,8,2048]{2,1,0:T(8,128)(2,1)S(1)}, u32[]{:S(2)}, u32[]{:S(2)}) collective-permute-start(bf16[4,8,2048]{2,1,0:T(8,128)(2,1)} %dynamic-slice_bitcast_fusion.3), channel_id=1, source_target_pairs={{0,240},{8,248},{16,0},{24,8},{32,16},{40,24},{48,32},{56,40},{64,... | collective-permute-start | bytes 393224 | tf_op jit(solution)/shard_map/ppermute | solution.py:76
  138.4 16.6 %collective-permute-start.7 = (bf16[4,8,2048]{2,1,0:T(8,128)(2,1)}, bf16[4,8,2048]{2,1,0:T(8,128)(2,1)}, u32[]{:S(2)}, u32[]{:S(2)}) collective-permute-start(bf16[4,8,2048]{2,1,0:T(8,128)(2,1)} %slice_bitcast_fusion.2), channel_id=1, source_target_pairs={{0,16},{8,24},{16,32},{24,40},{32,48},{40,56},{48,64},{56,72},{64,... | collective-permute-start | bytes 393224 | tf_op jit(solution)/shard_map/ppermute | solution.py:76
  156.8 48.9 %all-to-all-start.3 = ((bf16[8,8,2048]{2,1,0:T(8,128)(2,1)}), bf16[8,8,2048]{2,1,0:T(8,128)(2,1)S(1)}, u32[]{:S(2)}, u32[]{:S(2)}) async-start(bf16[8,8,2048]{2,1,0:T(8,128)(2,1)} %fusion.5), calls=%async_computation.3 | async-start | bytes 524288 | tf_op jit(solution)/shard_map/all_to_all | solution.py:28
  218.1 43.3 %collective-permute-start.13 = (bf16[2,2048,128]{2,1,0:T(8,128)(2,1)}, bf16[2,2048,128]{2,1,0:T(8,128)(2,1)S(1)}, u32[]{:S(2)}, u32[]{:S(2)}) collective-permute-start(bf16[2,2048,128]{2,1,0:T(8,128)(2,1)} %pad_maximum_fusion.2), channel_id=1, source_target_pairs={{0,1},{8,9},{16,17},{24,25},{33,32},{41,40},{49,48},{57,56},{66,67... | collective-permute-start | bytes 3145736 | tf_op jit(solution)/shard_map/ppermute | solution.py:136
  251.8 9.6 %all-to-all-start.6 = ((f32[8,8,256]{2,1,0:T(8,128)}), f32[8,8,256]{2,1,0:T(8,128)S(1)}, u32[]{:S(2)}, u32[]{:S(2)}) async-start(f32[8,8,256]{2,1,0:T(8,128)} %bitcast.118), calls=%async_computation.6 | async-start | bytes 131072 | tf_op jit(solution)/shard_map/all_to_all | solution.py:28
  261.4 22.5 %copy-start.1 = (bf16[2,2048,128]{2,1,0:T(8,128)(2,1)}, bf16[2,2048,128]{2,1,0:T(8,128)(2,1)S(1)}, u32[]{:S(2)}) copy-start(bf16[2,2048,128]{2,1,0:T(8,128)(2,1)S(1)} %collective-permute-done.13) | copy-start | bytes 3145732
  262.7 24.7 %collective-permute-start.14 = (bf16[2,2048,128]{2,1,0:T(8,128)(2,1)}, bf16[2,2048,128]{2,1,0:T(8,128)(2,1)}, u32[]{:S(2)}, u32[]{:S(2)}) collective-permute-start(bf16[2,2048,128]{2,1,0:T(8,128)(2,1)} %broadcast_select_fusion), channel_id=1, source_target_pairs={{0,2},{1,3},{8,10},{9,11},{16,18},{17,19},{24,26},{25,27},{32,34},... | collective-permute-start | bytes 3145736 | tf_op jit(solution)/shard_map/ppermute | solution.py:136
  264.3 23.1 %collective-permute-start.15 = (bf16[2,2048,128]{2,1,0:T(8,128)(2,1)}, bf16[2,2048,128]{2,1,0:T(8,128)(2,1)}, u32[]{:S(2)}, u32[]{:S(2)}) collective-permute-start(bf16[2,2048,128]{2,1,0:T(8,128)(2,1)} %broadcast_select_fusion), channel_id=1, source_target_pairs={{0,6},{1,7},{8,14},{9,15},{16,22},{17,23},{24,30},{25,31},{32,38},... | collective-permute-start | bytes 3145736 | tf_op jit(solution)/shard_map/ppermute | solution.py:136
  267.5 48.1 %all-to-all-start.7 = ((bf16[8,8,2048]{2,1,0:T(8,128)(2,1)}), bf16[8,8,2048]{2,1,0:T(8,128)(2,1)S(1)}, u32[]{:S(2)}, u32[]{:S(2)}) async-start(bf16[8,8,2048]{2,1,0:T(8,128)(2,1)} %broadcast_in_dim.59), calls=%async_computation.7 | async-start | bytes 524288 | tf_op jit(solution)/shard_map/all_to_all | solution.py:28
  285.0 2.4 copy-start.2
  289.9 59.6 %collective-permute-start.17 = (bf16[2048,128]{1,0:T(8,128)(2,1)}, bf16[2048,128]{1,0:T(8,128)(2,1)S(1)}, u32[]{:S(2)}, u32[]{:S(2)}) collective-permute-start(bf16[2048,128]{1,0:T(8,128)(2,1)} %get-tuple-element.32), channel_id=1, source_target_pairs={{6,4},{7,5},{14,12},{15,13},{22,20},{23,21},{30,28},{31,29},{38,36... | collective-permute-start | bytes 1572872 | tf_op jit(solution)/shard_map/ppermute | solution.py:136
  291.2 58.3 %collective-permute-start.16 = (bf16[2048,128]{1,0:T(8,128)(2,1)}, bf16[2048,128]{1,0:T(8,128)(2,1)S(1)}, u32[]{:S(2)}, u32[]{:S(2)}) collective-permute-start(bf16[2048,128]{1,0:T(8,128)(2,1)} %get-tuple-element.33), channel_id=1, source_target_pairs={{2,4},{3,5},{10,12},{11,13},{18,20},{19,21},{26,28},{27,29},{34,36... | collective-permute-start | bytes 1572872 | tf_op jit(solution)/shard_map/ppermute | solution.py:136
  315.6 27.4 %collective-permute-start.11 = (bf16[4,8,2048]{2,1,0:T(8,128)(2,1)S(1)}, bf16[4,8,2048]{2,1,0:T(8,128)(2,1)S(1)}, u32[]{:S(2)}, u32[]{:S(2)}) collective-permute-start(bf16[4,8,2048]{2,1,0:T(8,128)(2,1)S(1)} %get-tuple-element.44), channel_id=1, source_target_pairs={{0,240},{8,248},{16,0},{24,8},{32,16},{40,24},{48,32},{56,40},{64,... | collective-permute-start | bytes 393224 | tf_op jit(solution)/shard_map/ppermute | solution.py:76
  328.6 14.3 %collective-permute-start.10 = (bf16[4,8,2048]{2,1,0:T(8,128)(2,1)S(1)}, bf16[4,8,2048]{2,1,0:T(8,128)(2,1)S(1)}, u32[]{:S(2)}, u32[]{:S(2)}) collective-permute-start(bf16[4,8,2048]{2,1,0:T(8,128)(2,1)S(1)} %get-tuple-element.43), channel_id=1, source_target_pairs={{0,16},{8,24},{16,32},{24,40},{32,48},{40,56},{48,64},{56,72},{64,... | collective-permute-start | bytes 393224 | tf_op jit(solution)/shard_map/ppermute | solution.py:76
  330.6 8.9 %collective-permute-start.9 = (bf16[8,8,2048]{2,1,0:T(8,128)(2,1)S(1)}, bf16[8,8,2048]{2,1,0:T(8,128)(2,1)S(1)}, u32[]{:S(2)}, u32[]{:S(2)}) collective-permute-start(bf16[8,8,2048]{2,1,0:T(8,128)(2,1)S(1)} %all-to-all-done.7), channel_id=1, source_target_pairs={{0,248},{8,0},{16,8},{24,16},{32,24},{40,32},{48,40},{56,48},{64,5... | collective-permute-start | bytes 786440 | tf_op jit(solution)/shard_map/ppermute | solution.py:76
  339.5 10.0 %collective-permute-start.12 = (bf16[8,8,2048]{2,1,0:T(8,128)(2,1)S(1)}, bf16[8,8,2048]{2,1,0:T(8,128)(2,1)S(1)}, u32[]{:S(2)}, u32[]{:S(2)}) collective-permute-start(bf16[8,8,2048]{2,1,0:T(8,128)(2,1)S(1)} %all-to-all-done.7), channel_id=1, source_target_pairs={{0,8},{8,16},{16,24},{24,32},{32,40},{40,48},{48,56},{56,64},{64,7... | collective-permute-start | bytes 786440 | tf_op jit(solution)/shard_map/ppermute | solution.py:76
  349.5 1.3 copy-start.4
Sparse Core Ops, SparseCore 0:
  10.7 204.3 all-gather.1

commit v2 on v1

--- a/solution.py
+++ b/solution.py
@@ -110,7 +110,8 @@
     me = lax.axis_index("fs")
     far, rows, width = got.shape
     h = far // 2
-    ahead, behind = shift(got, -1), shift(got, 1)
+    ahead = shift(got, -1)
+    behind = shift(got, 1)
     low, high = shift(got[:h], 2), shift(got[h:], -2)
     out = jnp.zeros((far, NEAR, rows, width), got.dtype)
     pieces = (got, ahead, jnp.concatenate([low, high], axis=0), behind)
@@ -124,6 +125,7 @@
     chips = n_tp // 2
     per = n // n_tp
     me, t = lax.axis_index("fs"), lax.axis_index("tp")
+    core = t % 2
     planes, _, cols = whole.shape
     lanes = cols * 2 // per
     home = me // per
@@ -138,24 +140,29 @@
     def first():
         half = me % per // 2 * rows
         both = [lax.dynamic_slice(whole, (0, 2 * m * rows + half, 0), (planes, rows, cols)) for m in range(2)]
-        both = [jnp.where(me % 2 == 0, w[..., :lanes], w[..., lanes:]) for w in both]
-        return jnp.stack([w.reshape(planes * rows, lanes) for w in both])
-
-    def second(array):
-        other = hop(array, lambda f: [(f * n_tp + f // per, f * n_tp + (f // per ^ 1))])
-        return lambda: jnp.where(t == home, array, other)
-
-    def third(array):
-        up = hop(array, lambda f: [(at(f, 0, c), at(f, 1, c)) for c in range(2)])
-        down = hop(array, lambda f: [(at(f, 0, c), at(f, -1, c)) for c in range(2)])
-        return lambda: jnp.where(ahead == 0, array, jnp.where(ahead == 1, up, down))
-
-    def fourth(array):
-        gate = hop(array[0], lambda f: [(at(f, 1, c), at(f, 2, c)) for c in range(2)])
-        up = hop(array[1], lambda f: [(at(f, -1, c), at(f, -2, c)) for c in range(2)])
-        return lambda: (jnp.where(ahead == 2, gate, array[0]), jnp.where(ahead == 2, up, array[1]))
-
-    return first, second, third, fourth
+        both = [jnp.where(me % 2 == 0, w[..., :lanes], w[..., lanes:]).reshape(planes * rows, lanes) for w in both]
+        return jnp.where(core == 0, both[0], both[1]), jnp.where(core == 0, both[1], both[0])
+
+    def second(mine, theirs):
+        other = hop(theirs, lambda f: [(f * n_tp + f // per, f * n_tp + (f // per ^ 1))])
+        return lambda: jnp.where(t == home, mine, other)
+
+    def third(mine):
+        up = hop(mine, lambda f: [(at(f, 0, c), at(f, 1, c)) for c in range(2)])
+        down = hop(mine, lambda f: [(at(f, 0, c), at(f, -1, c)) for c in range(2)])
+        return lambda: jnp.where(ahead == 0, mine, jnp.where(ahead == 1, up, down))
+
+    def fourth(mine):
+        h = mine.shape[0] // 2
+        low = hop(mine[:h], lambda f: [(at(f, 1, c), at(f, 2, c)) for c in range(2)])
+        high = hop(mine[h:], lambda f: [(at(f, -1, c), at(f, -2, c)) for c in range(2)])
+        return lambda: jnp.where(ahead == 2, jnp.concatenate([low, high], axis=0), mine)
+
+    def fifth(mine):
+        other = hop(mine, lambda f: [(f * n_tp + t, f * n_tp + (t ^ 1)) for t in range(n_tp)])
+        return lambda: (jnp.where(core == 0, mine, other), jnp.where(core == 0, other, mine))
+
+    return first, second, third, fourth, fifth
 
 
 STEPS = 4
@@ -300,10 +307,10 @@
 
     normed = spread_copies(normed_of(own), "tp", n_tp).reshape(n_tp * tokens, width)
     hidden = hidden_kernel(normed, whole)
-    step1, step2, step3, step4 = cast_in_plane(whole, rows)
+    step1, step2, step3, step4, step5 = cast_in_plane(whole, rows)
     hidden = spread_copies(hidden, "tp", n_tp)
     cast = step1()
-    done = step2(cast)
+    done = step2(*cast)
     out = down_kernel(hidden, whole, hid)
     out = exchange(out.reshape(n_tp, tokens, dcols), "tp")
     cast = done()
@@ -312,8 +319,10 @@
     got = spread_far(own.astype(BF16))
     cast = done()
     done = step4(cast)
+    result = gather_near(got)
+    cast = done()
+    done = step5(cast)
     gate_served, up_served = done()
-    result = gather_near(got)
     return (result, first[0], first[1], first[2], gate_served, up_served, down_second_served)
 
 

time: 359 us -> 338 us (0.942)
  the two profiles are of different devices: /device:TPU:36 before, /device:TPU:44 now
where the time goes in v2:
time: 338 us; the launch traced here: 336 us
  starting transfers between devices  148 us (44%)
  waiting for transfers between devices  128 us (38%)
  between operations  14.8 us (4%)
  local copies, waits for them, and re-layouts  13.3 us (4%)
  other arithmetic  13.3 us (4%)
  blocking collectives  9.99 us (3%)
  Pallas kernels  7.78 us (2%)
    all_to_all x7, waiting for transfers between devices, exchange(): lax.all_to_all(blocks, axis, split_axis=0, concat_axis=0, tiled=True, axi...  96 us
    all_to_all x7, starting transfers between devices, exchange(): lax.all_to_all(blocks, axis, split_axis=0, concat_axis=0, tiled=True, axi...  90.3 us
    ppermute x8, starting transfers between devices, shift(): return lax.ppermute(array, 'fs', [(i, (i + steps) % n) for i in range(n)])  34.6 us
    ppermute x8, waiting for transfers between devices, shift(): return lax.ppermute(array, 'fs', [(i, (i + steps) % n) for i in range(n)])  18.8 us
    ppermute x3, starting transfers between devices, shift_tp(): return lax.ppermute(array, 'tp', [(i, (i + steps) % n) for i in range(n)])  11.2 us
    all_to_all x1, blocking collectives, exchange(): lax.all_to_all(blocks, axis, split_axis=0, concat_axis=0, tiled=True, axi...  9.99 us
    ppermute x6, waiting for transfers between devices, hop(): lax.ppermute(array, ('fs', 'tp'), [pair for f in range(n) for pair in pai...  8.4 us
    ppermute x6, starting transfers between devices, hop(): lax.ppermute(array, ('fs', 'tp'), [pair for f in range(n) for pair in pai...  7.55 us
  transfers between devices with their start and end apart: 27, of which 15 were waited for; matrix products, arithmetic and copies ran while one was open for 7% of the time, Pallas kernels for 2%

profile of v2, /device:TPU:44, one launch (start us, length us, event | category | flops | bytes accessed | tf_op | source)
XLA Modules:
  0.0 336.2 jit_solution(10551720721669774159)
XLA Ops:
  7.3 1.1 multiply_convert_fusion
  10.0 1.1 fusion.16
  11.8 4.8 %all-to-all-start = ((bf16[8,2,8,512]{3,2,1,0:T(8,128)(2,1)}), bf16[8,2,8,512]{3,2,1,0:T(8,128)(2,1)S(1)}, u32[]{:S(2)}, u32[]{:S(2)}) async-start(bf16[8,2,8,512]{3,2,1,0:T(8,128)(2,1)} %maximum_bitcast_fusion.1), calls=%async_computation | async-start | bytes 262144 | tf_op jit(solution)/shard_map/all_to_all | solution.py:28
  16.6 3.4 %all-to-all-done = bf16[8,2,8,512]{3,2,1,0:T(8,128)(2,1)S(1)} async-done(((bf16[8,2,8,512]{3,2,1,0:T(8,128)(2,1)}), bf16[8,2,8,512]{3,2,1,0:T(8,128)(2,1)S(1)}, u32[]{:S(2)}, u32[]{:S(2)}) %all-to-all-start) | async-done | bytes 131104 | tf_op jit(solution)/shard_map/all_to_all | solution.py:28
  20.7 3.8 %collective-permute-start = (bf16[512,128]{1,0:T(8,128)(2,1)S(1)}, bf16[512,128]{1,0:T(8,128)(2,1)S(1)}, u32[]{:S(2)}, u32[]{:S(2)}) collective-permute-start(bf16[512,128]{1,0:T(8,128)(2,1)S(1)} %pad_maximum_fusion.3), channel_id=1, source_target_pairs={{0,6},{1,7},{2,0},{3,1},{4,2},{5,3},{6,4},{7,5},{8,14},{9,15},{10,... | collective-permute-start | bytes 393224 | tf_op jit(solution)/shard_map/ppermute | solution.py:57
  24.6 4.0 %collective-permute-start.1 = (bf16[512,128]{1,0:T(8,128)(2,1)S(1)}, bf16[512,128]{1,0:T(8,128)(2,1)S(1)}, u32[]{:S(2)}, u32[]{:S(2)}) collective-permute-start(bf16[512,128]{1,0:T(8,128)(2,1)S(1)} %pad_maximum_fusion.3), channel_id=1, source_target_pairs={{0,4},{1,5},{2,6},{3,7},{4,0},{5,1},{6,2},{7,3},{8,12},{9,13},{10,... | collective-permute-start | bytes 393224 | tf_op jit(solution)/shard_map/ppermute | solution.py:57
  28.6 3.4 %collective-permute-start.2 = (bf16[512,128]{1,0:T(8,128)(2,1)S(1)}, bf16[512,128]{1,0:T(8,128)(2,1)S(1)}, u32[]{:S(2)}, u32[]{:S(2)}) collective-permute-start(bf16[512,128]{1,0:T(8,128)(2,1)S(1)} %pad_maximum_fusion.3), channel_id=1, source_target_pairs={{0,2},{1,3},{2,4},{3,5},{4,6},{5,7},{6,0},{7,1},{8,10},{9,11},{10,... | collective-permute-start | bytes 393224 | tf_op jit(solution)/shard_map/ppermute | solution.py:57
  32.0 45.8 %all-to-all-start.1 = ((bf16[32,2,8,128]{3,2,1,0:T(8,128)(2,1)}), bf16[32,2,8,128]{3,2,1,0:T(8,128)(2,1)S(1)}, u32[]{:S(2)}, u32[]{:S(2)}) async-start(bf16[32,2,8,128]{3,2,1,0:T(8,128)(2,1)} %bitcast.3), calls=%async_computation.1 | async-start | bytes 262144 | tf_op jit(solution)/shard_map/all_to_all | solution.py:28
  78.0 2.0 collective-permute-start.3
  80.0 1.9 collective-permute-done.3
  82.1 27.9 %all-to-all-done.1 = bf16[32,2,8,128]{3,2,1,0:T(8,128)(2,1)S(1)} async-done(((bf16[32,2,8,128]{3,2,1,0:T(8,128)(2,1)}), bf16[32,2,8,128]{3,2,1,0:T(8,128)(2,1)S(1)}, u32[]{:S(2)}, u32[]{:S(2)}) %all-to-all-start.1) | async-done | bytes 131104 | tf_op jit(solution)/shard_map/all_to_all | solution.py:28
  110.0 10.0 %all_to_all.40 = bf16[4,512,128]{2,1,0:T(8,128)(2,1)S(1)} all-to-all(bf16[4,512,128]{2,1,0:T(8,128)(2,1)S(1)} %broadcast_in_dim.56), channel_id=1, replica_groups={{0,2,4,6},{1,3,5,7},{8,10,12,14},{9,11,13,15},{16,18,20,22},{17,19,21,2..., dimensions={0} | all-to-all | bytes 1048576 | tf_op jit(solution)/shard_map/all_to_all | solution.py:28
  120.0 1.9 collective-permute-start.4
  124.0 1.1 select_bitcast_fusion.1
  128.3 1.9 collective-permute-start.6
  130.2 4.0 %collective-permute-start.5 = (bf16[8,8,2048]{2,1,0:T(8,128)(2,1)S(1)}, bf16[8,8,2048]{2,1,0:T(8,128)(2,1)S(1)}, u32[]{:S(2)}, u32[]{:S(2)}) collective-permute-start(bf16[8,8,2048]{2,1,0:T(8,128)(2,1)S(1)} %get-tuple-element.34), channel_id=1, source_target_pairs={{0,8},{8,16},{16,24},{24,32},{32,40},{40,48},{48,56},{56,64},{64,7... | collective-permute-start | bytes 786440 | tf_op jit(solution)/shard_map/ppermute | solution.py:76
  134.9 2.4 collective-permute-start.8
  137.9 4.4 %collective-permute-start.7 = (bf16[4,8,2048]{2,1,0:T(8,128)(2,1)}, bf16[4,8,2048]{2,1,0:T(8,128)(2,1)}, u32[]{:S(2)}, u32[]{:S(2)}) collective-permute-start(bf16[4,8,2048]{2,1,0:T(8,128)(2,1)} %slice_bitcast_fusion), channel_id=1, source_target_pairs={{0,16},{8,24},{16,32},{24,40},{32,48},{40,56},{48,64},{56,72},{64,... | collective-permute-start | bytes 393224 | tf_op jit(solution)/shard_map/ppermute | solution.py:76
  142.3 9.3 %collective-permute-done.8 = bf16[4,8,2048]{2,1,0:T(8,128)(2,1)S(1)} collective-permute-done((bf16[4,8,2048]{2,1,0:T(8,128)(2,1)}, bf16[4,8,2048]{2,1,0:T(8,128)(2,1)S(1)}, u32[]{:S(2)}, u32[]{:S(2)}) %collective-permute-start.8) | collective-permute-done | bytes 131104 | tf_op jit(solution)/shard_map/ppermute | solution.py:76
  151.6 2.7 collective-permute-done.7
  154.3 1.7 fusion.5
  156.0 5.1 %all-to-all-start.3 = ((bf16[8,8,2048]{2,1,0:T(8,128)(2,1)}), bf16[8,8,2048]{2,1,0:T(8,128)(2,1)S(1)}, u32[]{:S(2)}, u32[]{:S(2)}) async-start(bf16[8,8,2048]{2,1,0:T(8,128)(2,1)} %fusion.5), calls=%async_computation.3 | async-start | bytes 524288 | tf_op jit(solution)/shard_map/all_to_all | solution.py:28
  161.2 43.5 %all-to-all-done.3 = bf16[8,8,2048]{2,1,0:T(8,128)(2,1)S(1)} async-done(((bf16[8,8,2048]{2,1,0:T(8,128)(2,1)}), bf16[8,8,2048]{2,1,0:T(8,128)(2,1)S(1)}, u32[]{:S(2)}, u32[]{:S(2)}) %all-to-all-start.3) | async-done | bytes 262176 | tf_op jit(solution)/shard_map/all_to_all | solution.py:28
  205.7 6.0 %all-to-all-start.4 = ((bf16[8,8,2048]{2,1,0:T(8,128)(2,1)}), bf16[8,8,2048]{2,1,0:T(8,128)(2,1)S(1)}, u32[]{:S(2)}, u32[]{:S(2)}) async-start(bf16[8,8,2048]{2,1,0:T(8,128)(2,1)} %broadcast_in_dim.57), calls=%async_computation.4 | async-start | bytes 524288 | tf_op jit(solution)/shard_map/all_to_all | solution.py:28
  211.7 2.6 all-gather.2.cloned.1.call-done
  214.3 2.8 broadcast_select_fusion.1
  218.4 4.2 %hidden_second.1 = bf16[64,512]{1,0:T(8,128)(2,1)} custom-call(bf16[64,2048]{1,0:T(8,128)(2,1)} %bitcast.100, bf16[32,384,256]{2,1,0:T(8,128)(2,1)} %bitcast.86), custom_call_target="tpu_custom_call" | custom-call | tf_op jit(solution)/shard_map/hidden_second/pallas_call | solution.py:200
  222.7 1.7 broadcast_in_dim.58
  224.3 5.1 %all-to-all-start.5 = ((bf16[8,64,512]{2,1,0:T(8,128)(2,1)}), bf16[8,64,512]{2,1,0:T(8,128)(2,1)S(1)}, u32[]{:S(2)}, u32[]{:S(2)}) async-start(bf16[8,64,512]{2,1,0:T(8,128)(2,1)} %broadcast_in_dim.58), calls=%async_computation.5 | async-start | bytes 1048576 | tf_op jit(solution)/shard_map/all_to_all | solution.py:28
  229.4 7.1 %all-to-all-done.5.h_ref = bf16[8,64,512]{2,1,0:T(8,128)(2,1)S(1)} async-done(((bf16[8,64,512]{2,1,0:T(8,128)(2,1)}), bf16[8,64,512]{2,1,0:T(8,128)(2,1)S(1)}, u32[]{:S(2)}, u32[]{:S(2)}) %all-to-all-start.5) | async-done | bytes 524320 | tf_op jit(solution)/shard_map/all_to_all | solution.py:28
  237.3 3.6 %down_second.1 = f32[64,256]{1,0:T(8,128)} custom-call(bf16[8,64,512]{2,1,0:T(8,128)(2,1)} %copy-done.3, bf16[32,384,256]{2,1,0:T(8,128)(2,1)} %bitcast.87), custom_call_target="tpu_custom_call" | custom-call | tf_op jit(solution)/shard_map/down_second/pallas_call | solution.py:232
  240.9 6.5 %all-to-all-start.6 = ((f32[8,8,256]{2,1,0:T(8,128)}), f32[8,8,256]{2,1,0:T(8,128)S(1)}, u32[]{:S(2)}, u32[]{:S(2)}) async-start(f32[8,8,256]{2,1,0:T(8,128)} %bitcast.105), calls=%async_computation.6 | async-start | bytes 131072 | tf_op jit(solution)/shard_map/all_to_all | solution.py:28
  248.2 1.5 collective-permute-start.15
  251.3 16.9 %all-to-all-start.7 = ((bf16[8,8,2048]{2,1,0:T(8,128)(2,1)}), bf16[8,8,2048]{2,1,0:T(8,128)(2,1)S(1)}, u32[]{:S(2)}, u32[]{:S(2)}) async-start(bf16[8,8,2048]{2,1,0:T(8,128)(2,1)} %broadcast_in_dim.59), calls=%async_computation.7 | async-start | bytes 524288 | tf_op jit(solution)/shard_map/all_to_all | solution.py:28
  268.2 1.1 select_select_fusion
  269.4 1.4 collective-permute-start.17
  270.9 1.3 collective-permute-start.16
  272.2 7.1 %collective-permute-done.17 = bf16[1024,128]{1,0:T(8,128)(2,1)S(1)} collective-permute-done((bf16[1024,128]{1,0:T(8,128)(2,1)S(1)}, bf16[1024,128]{1,0:T(8,128)(2,1)S(1)}, u32[]{:S(2)}, u32[]{:S(2)}) %collective-permute-start.17) | collective-permute-done | bytes 262176 | tf_op jit(solution)/shard_map/ppermute | solution.py:138
  279.3 1.3 collective-permute-done.16
  280.7 2.0 collective-permute-start.18
  285.0 1.0 broadcast_select_fusion.2
  286.0 13.2 %all-to-all-done.7 = bf16[8,8,2048]{2,1,0:T(8,128)(2,1)S(1)} async-done(((bf16[8,8,2048]{2,1,0:T(8,128)(2,1)}), bf16[8,8,2048]{2,1,0:T(8,128)(2,1)S(1)}, u32[]{:S(2)}, u32[]{:S(2)}) %all-to-all-start.7) | async-done | bytes 262176 | tf_op jit(solution)/shard_map/all_to_all | solution.py:28
  299.3 12.9 %collective-permute-start.11 = (bf16[4,8,2048]{2,1,0:T(8,128)(2,1)S(1)}, bf16[4,8,2048]{2,1,0:T(8,128)(2,1)S(1)}, u32[]{:S(2)}, u32[]{:S(2)}) collective-permute-start(bf16[4,8,2048]{2,1,0:T(8,128)(2,1)S(1)} %get-tuple-element.44), channel_id=1, source_target_pairs={{0,240},{8,248},{16,0},{24,8},{32,16},{40,24},{48,32},{56,40},{64,... | collective-permute-start | bytes 393224 | tf_op jit(solution)/shard_map/ppermute | solution.py:76
  312.2 3.2 collective-permute-start.10
  315.4 2.5 collective-permute-start.9
  317.9 3.4 %collective-permute-start.12 = (bf16[8,8,2048]{2,1,0:T(8,128)(2,1)S(1)}, bf16[8,8,2048]{2,1,0:T(8,128)(2,1)S(1)}, u32[]{:S(2)}, u32[]{:S(2)}) collective-permute-start(bf16[8,8,2048]{2,1,0:T(8,128)(2,1)S(1)} %all-to-all-done.7), channel_id=1, source_target_pairs={{0,8},{8,16},{16,24},{24,32},{32,40},{40,48},{48,56},{56,64},{64,7... | collective-permute-start | bytes 786440 | tf_op jit(solution)/shard_map/ppermute | solution.py:76
  321.4 3.7 %collective-permute-done.9 = bf16[8,8,2048]{2,1,0:T(8,128)(2,1)S(1)} collective-permute-done((bf16[8,8,2048]{2,1,0:T(8,128)(2,1)S(1)}, bf16[8,8,2048]{2,1,0:T(8,128)(2,1)S(1)}, u32[]{:S(2)}, u32[]{:S(2)}) %collective-permute-start.9) | collective-permute-done | bytes 262176 | tf_op jit(solution)/shard_map/ppermute | solution.py:76
  325.2 3.1 collective-permute-done.12
  (89 shorter events, 19.2 us)
Async XLA Ops:
  7.2 9.4 %copy-start.8 = (f32[128,256]{1,0:T(8,128)S(1)}, f32[128,256]{1,0:T(8,128)}, u32[]{:S(2)}) copy-start(f32[128,256]{1,0:T(8,128)} %param.13) | copy-start | bytes 393220
  7.2 207.1 %all-gather.2.cloned.1.call-start = ((), (), s32[]{:S(2)}) async-start(), calls=%async_computation.8 | async-start | bytes 6488064 | tf_op jit(solution)/shard_map/all_gather | solution.py:268
  9.3 0.7 copy-start.7
  11.8 8.2 %all-to-all-start = ((bf16[8,2,8,512]{3,2,1,0:T(8,128)(2,1)}), bf16[8,2,8,512]{3,2,1,0:T(8,128)(2,1)S(1)}, u32[]{:S(2)}, u32[]{:S(2)}) async-start(bf16[8,2,8,512]{3,2,1,0:T(8,128)(2,1)} %maximum_bitcast_fusion.1), calls=%async_computation | async-start | bytes 262144 | tf_op jit(solution)/shard_map/all_to_all | solution.py:28
  20.7 57.2 %collective-permute-start = (bf16[512,128]{1,0:T(8,128)(2,1)S(1)}, bf16[512,128]{1,0:T(8,128)(2,1)S(1)}, u32[]{:S(2)}, u32[]{:S(2)}) collective-permute-start(bf16[512,128]{1,0:T(8,128)(2,1)S(1)} %pad_maximum_fusion.3), channel_id=1, source_target_pairs={{0,6},{1,7},{2,0},{3,1},{4,2},{5,3},{6,4},{7,5},{8,14},{9,15},{10,... | collective-permute-start | bytes 393224 | tf_op jit(solution)/shard_map/ppermute | solution.py:57
  24.6 53.4 %collective-permute-start.1 = (bf16[512,128]{1,0:T(8,128)(2,1)S(1)}, bf16[512,128]{1,0:T(8,128)(2,1)S(1)}, u32[]{:S(2)}, u32[]{:S(2)}) collective-permute-start(bf16[512,128]{1,0:T(8,128)(2,1)S(1)} %pad_maximum_fusion.3), channel_id=1, source_target_pairs={{0,4},{1,5},{2,6},{3,7},{4,0},{5,1},{6,2},{7,3},{8,12},{9,13},{10,... | collective-permute-start | bytes 393224 | tf_op jit(solution)/shard_map/ppermute | solution.py:57
  28.6 49.4 %collective-permute-start.2 = (bf16[512,128]{1,0:T(8,128)(2,1)S(1)}, bf16[512,128]{1,0:T(8,128)(2,1)S(1)}, u32[]{:S(2)}, u32[]{:S(2)}) collective-permute-start(bf16[512,128]{1,0:T(8,128)(2,1)S(1)} %pad_maximum_fusion.3), channel_id=1, source_target_pairs={{0,2},{1,3},{2,4},{3,5},{4,6},{5,7},{6,0},{7,1},{8,10},{9,11},{10,... | collective-permute-start | bytes 393224 | tf_op jit(solution)/shard_map/ppermute | solution.py:57
  32.0 77.9 %all-to-all-start.1 = ((bf16[32,2,8,128]{3,2,1,0:T(8,128)(2,1)}), bf16[32,2,8,128]{3,2,1,0:T(8,128)(2,1)S(1)}, u32[]{:S(2)}, u32[]{:S(2)}) async-start(bf16[32,2,8,128]{3,2,1,0:T(8,128)(2,1)} %bitcast.3), calls=%async_computation.1 | async-start | bytes 262144 | tf_op jit(solution)/shard_map/all_to_all | solution.py:28
  78.0 3.8 %collective-permute-start.3 = (bf16[4,512,128]{2,1,0:T(8,128)(2,1)S(1)}, bf16[4,512,128]{2,1,0:T(8,128)(2,1)S(1)}, u32[]{:S(2)}, u32[]{:S(2)}) collective-permute-start(bf16[4,512,128]{2,1,0:T(8,128)(2,1)S(1)} %bitcast_dynamic-update-slice_fusion.3), channel_id=1, source_target_pairs={{0,1},{1,0},{2,3},{3,2},{4,5},{5,4},{6,7},{7,6},{8,9},{9,8},{10,11... | collective-permute-start | bytes 1572872 | tf_op jit(solution)/shard_map/ppermute | solution.py:68
  82.0 40.0 %copy-start = (bf16[256,2048]{1,0:T(8,128)(2,1)S(1)}, bf16[256,2048]{1,0:T(8,128)(2,1)}, u32[]{:S(2)}) copy-start(bf16[256,2048]{1,0:T(8,128)(2,1)} %param.9) | copy-start | bytes 3145732
  120.0 4.0 %collective-permute-start.4 = (bf16[4,512,128]{2,1,0:T(8,128)(2,1)S(1)}, bf16[4,512,128]{2,1,0:T(8,128)(2,1)}, u32[]{:S(2)}, u32[]{:S(2)}) collective-permute-start(bf16[4,512,128]{2,1,0:T(8,128)(2,1)S(1)} %all_to_all.40), channel_id=1, source_target_pairs={{0,1},{1,0},{2,3},{3,2},{4,5},{5,4},{6,7},{7,6},{8,9},{9,8},{10,11... | collective-permute-start | bytes 1572872 | tf_op jit(solution)/shard_map/ppermute | solution.py:49
  125.7 1.8 copy-start.1
  125.9 0.8 copy-start.6
  128.3 26.0 %collective-permute-start.6 = (bf16[8,8,2048]{2,1,0:T(8,128)(2,1)}, bf16[8,8,2048]{2,1,0:T(8,128)(2,1)S(1)}, u32[]{:S(2)}, u32[]{:S(2)}) collective-permute-start(bf16[8,8,2048]{2,1,0:T(8,128)(2,1)} %get-tuple-element.33), channel_id=1, source_target_pairs={{0,248},{8,0},{16,8},{24,16},{32,24},{40,32},{48,40},{56,48},{64,5... | collective-permute-start | bytes 786440 | tf_op jit(solution)/shard_map/ppermute | solution.py:76
  130.2 24.1 %collective-permute-start.5 = (bf16[8,8,2048]{2,1,0:T(8,128)(2,1)S(1)}, bf16[8,8,2048]{2,1,0:T(8,128)(2,1)S(1)}, u32[]{:S(2)}, u32[]{:S(2)}) collective-permute-start(bf16[8,8,2048]{2,1,0:T(8,128)(2,1)S(1)} %get-tuple-element.34), channel_id=1, source_target_pairs={{0,8},{8,16},{16,24},{24,32},{32,40},{40,48},{48,56},{56,64},{64,7... | collective-permute-start | bytes 786440 | tf_op jit(solution)/shard_map/ppermute | solution.py:76
  134.9 16.7 %collective-permute-start.8 = (bf16[4,8,2048]{2,1,0:T(8,128)(2,1)}, bf16[4,8,2048]{2,1,0:T(8,128)(2,1)S(1)}, u32[]{:S(2)}, u32[]{:S(2)}) collective-permute-start(bf16[4,8,2048]{2,1,0:T(8,128)(2,1)} %dynamic-slice_bitcast_fusion.3), channel_id=1, source_target_pairs={{0,240},{8,248},{16,0},{24,8},{32,16},{40,24},{48,32},{56,40},{64,... | collective-permute-start | bytes 393224 | tf_op jit(solution)/shard_map/ppermute | solution.py:76
  137.9 16.4 %collective-permute-start.7 = (bf16[4,8,2048]{2,1,0:T(8,128)(2,1)}, bf16[4,8,2048]{2,1,0:T(8,128)(2,1)}, u32[]{:S(2)}, u32[]{:S(2)}) collective-permute-start(bf16[4,8,2048]{2,1,0:T(8,128)(2,1)} %slice_bitcast_fusion), channel_id=1, source_target_pairs={{0,16},{8,24},{16,32},{24,40},{32,48},{40,56},{48,64},{56,72},{64,... | collective-permute-start | bytes 393224 | tf_op jit(solution)/shard_map/ppermute | solution.py:76
  156.0 48.6 %all-to-all-start.3 = ((bf16[8,8,2048]{2,1,0:T(8,128)(2,1)}), bf16[8,8,2048]{2,1,0:T(8,128)(2,1)S(1)}, u32[]{:S(2)}, u32[]{:S(2)}) async-start(bf16[8,8,2048]{2,1,0:T(8,128)(2,1)} %fusion.5), calls=%async_computation.3 | async-start | bytes 524288 | tf_op jit(solution)/shard_map/all_to_all | solution.py:28
  205.7 12.0 %all-to-all-start.4 = ((bf16[8,8,2048]{2,1,0:T(8,128)(2,1)}), bf16[8,8,2048]{2,1,0:T(8,128)(2,1)S(1)}, u32[]{:S(2)}, u32[]{:S(2)}) async-start(bf16[8,8,2048]{2,1,0:T(8,128)(2,1)} %broadcast_in_dim.57), calls=%async_computation.4 | async-start | bytes 524288 | tf_op jit(solution)/shard_map/all_to_all | solution.py:28
  217.0 30.4 %collective-permute-start.13 = (bf16[2048,128]{1,0:T(8,128)(2,1)}, bf16[2048,128]{1,0:T(8,128)(2,1)S(1)}, u32[]{:S(2)}, u32[]{:S(2)}) collective-permute-start(bf16[2048,128]{1,0:T(8,128)(2,1)} %bitcast.44), channel_id=1, source_target_pairs={{0,1},{8,9},{16,17},{24,25},{33,32},{41,40},{49,48},{57,56},{66,67... | collective-permute-start | bytes 1572872 | tf_op jit(solution)/shard_map/ppermute | solution.py:138
  217.7 0.7 copy-start.4
  224.3 12.2 %all-to-all-start.5 = ((bf16[8,64,512]{2,1,0:T(8,128)(2,1)}), bf16[8,64,512]{2,1,0:T(8,128)(2,1)S(1)}, u32[]{:S(2)}, u32[]{:S(2)}) async-start(bf16[8,64,512]{2,1,0:T(8,128)(2,1)} %broadcast_in_dim.58), calls=%async_computation.5 | async-start | bytes 1048576 | tf_op jit(solution)/shard_map/all_to_all | solution.py:28
  236.5 0.8 copy-start.3
  240.9 9.7 %all-to-all-start.6 = ((f32[8,8,256]{2,1,0:T(8,128)}), f32[8,8,256]{2,1,0:T(8,128)S(1)}, u32[]{:S(2)}, u32[]{:S(2)}) async-start(f32[8,8,256]{2,1,0:T(8,128)} %bitcast.105), calls=%async_computation.6 | async-start | bytes 131072 | tf_op jit(solution)/shard_map/all_to_all | solution.py:28
  247.5 20.7 %collective-permute-start.14 = (bf16[2048,128]{1,0:T(8,128)(2,1)S(1)}, bf16[2048,128]{1,0:T(8,128)(2,1)S(1)}, u32[]{:S(2)}, u32[]{:S(2)}) collective-permute-start(bf16[2048,128]{1,0:T(8,128)(2,1)S(1)} %bitcast_select_fusion), channel_id=1, source_target_pairs={{0,2},{1,3},{8,10},{9,11},{16,18},{17,19},{24,26},{25,27},{32,34},... | collective-permute-start | bytes 1572872 | tf_op jit(solution)/shard_map/ppermute | solution.py:138
  248.2 20.0 %collective-permute-start.15 = (bf16[2048,128]{1,0:T(8,128)(2,1)S(1)}, bf16[2048,128]{1,0:T(8,128)(2,1)}, u32[]{:S(2)}, u32[]{:S(2)}) collective-permute-start(bf16[2048,128]{1,0:T(8,128)(2,1)S(1)} %bitcast_select_fusion), channel_id=1, source_target_pairs={{0,6},{1,7},{8,14},{9,15},{16,22},{17,23},{24,30},{25,31},{32,38},... | collective-permute-start | bytes 1572872 | tf_op jit(solution)/shard_map/ppermute | solution.py:138
  251.3 48.0 %all-to-all-start.7 = ((bf16[8,8,2048]{2,1,0:T(8,128)(2,1)}), bf16[8,8,2048]{2,1,0:T(8,128)(2,1)S(1)}, u32[]{:S(2)}, u32[]{:S(2)}) async-start(bf16[8,8,2048]{2,1,0:T(8,128)(2,1)} %broadcast_in_dim.59), calls=%async_computation.7 | async-start | bytes 524288 | tf_op jit(solution)/shard_map/all_to_all | solution.py:28
  269.4 14.3 %copy-start.2 = (bf16[8,256,128]{2,1,0:T(8,128)(2,1)S(1)}, bf16[8,256,128]{2,1,0:T(8,128)(2,1)}, u32[]{:S(2)}) copy-start(bf16[8,256,128]{2,1,0:T(8,128)(2,1)} %get-tuple-element.28) | copy-start | bytes 1572868
  269.4 9.8 %collective-permute-start.17 = (bf16[1024,128]{1,0:T(8,128)(2,1)S(1)}, bf16[1024,128]{1,0:T(8,128)(2,1)S(1)}, u32[]{:S(2)}, u32[]{:S(2)}) collective-permute-start(bf16[1024,128]{1,0:T(8,128)(2,1)S(1)} %get-tuple-element.42), channel_id=1, source_target_pairs={{6,4},{7,5},{14,12},{15,13},{22,20},{23,21},{30,28},{31,29},{38,36... | collective-permute-start | bytes 786440 | tf_op jit(solution)/shard_map/ppermute | solution.py:138
  270.9 9.7 %collective-permute-start.16 = (bf16[1024,128]{1,0:T(8,128)(2,1)S(1)}, bf16[1024,128]{1,0:T(8,128)(2,1)S(1)}, u32[]{:S(2)}, u32[]{:S(2)}) collective-permute-start(bf16[1024,128]{1,0:T(8,128)(2,1)S(1)} %get-tuple-element.41), channel_id=1, source_target_pairs={{2,4},{3,5},{10,12},{11,13},{18,20},{19,21},{26,28},{27,29},{34,36... | collective-permute-start | bytes 786440 | tf_op jit(solution)/shard_map/ppermute | solution.py:138
  280.7 4.3 %collective-permute-start.18 = (bf16[2048,128]{1,0:T(8,128)(2,1)S(1)}, bf16[2048,128]{1,0:T(8,128)(2,1)S(1)}, u32[]{:S(2)}, u32[]{:S(2)}) collective-permute-start(bf16[2048,128]{1,0:T(8,128)(2,1)S(1)} %maximum_select_fusion), channel_id=1, source_target_pairs={{0,1},{1,0},{2,3},{3,2},{4,5},{5,4},{6,7},{7,6},{8,9},{9,8},{10,11... | collective-permute-start | bytes 1572872 | tf_op jit(solution)/shard_map/ppermute | solution.py:138
  299.3 25.9 %collective-permute-start.11 = (bf16[4,8,2048]{2,1,0:T(8,128)(2,1)S(1)}, bf16[4,8,2048]{2,1,0:T(8,128)(2,1)S(1)}, u32[]{:S(2)}, u32[]{:S(2)}) collective-permute-start(bf16[4,8,2048]{2,1,0:T(8,128)(2,1)S(1)} %get-tuple-element.44), channel_id=1, source_target_pairs={{0,240},{8,248},{16,0},{24,8},{32,16},{40,24},{48,32},{56,40},{64,... | collective-permute-start | bytes 393224 | tf_op jit(solution)/shard_map/ppermute | solution.py:76
  312.2 13.0 %collective-permute-start.10 = (bf16[4,8,2048]{2,1,0:T(8,128)(2,1)S(1)}, bf16[4,8,2048]{2,1,0:T(8,128)(2,1)S(1)}, u32[]{:S(2)}, u32[]{:S(2)}) collective-permute-start(bf16[4,8,2048]{2,1,0:T(8,128)(2,1)S(1)} %get-tuple-element.43), channel_id=1, source_target_pairs={{0,16},{8,24},{16,32},{24,40},{32,48},{40,56},{48,64},{56,72},{64,... | collective-permute-start | bytes 393224 | tf_op jit(solution)/shard_map/ppermute | solution.py:76
  315.4 9.8 %collective-permute-start.9 = (bf16[8,8,2048]{2,1,0:T(8,128)(2,1)S(1)}, bf16[8,8,2048]{2,1,0:T(8,128)(2,1)S(1)}, u32[]{:S(2)}, u32[]{:S(2)}) collective-permute-start(bf16[8,8,2048]{2,1,0:T(8,128)(2,1)S(1)} %all-to-all-done.7), channel_id=1, source_target_pairs={{0,248},{8,0},{16,8},{24,16},{32,24},{40,32},{48,40},{56,48},{64,5... | collective-permute-start | bytes 786440 | tf_op jit(solution)/shard_map/ppermute | solution.py:76
  317.9 10.4 %collective-permute-start.12 = (bf16[8,8,2048]{2,1,0:T(8,128)(2,1)S(1)}, bf16[8,8,2048]{2,1,0:T(8,128)(2,1)S(1)}, u32[]{:S(2)}, u32[]{:S(2)}) collective-permute-start(bf16[8,8,2048]{2,1,0:T(8,128)(2,1)S(1)} %all-to-all-done.7), channel_id=1, source_target_pairs={{0,8},{8,16},{16,24},{24,32},{32,40},{40,48},{48,56},{56,64},{64,7... | collective-permute-start | bytes 786440 | tf_op jit(solution)/shard_map/ppermute | solution.py:76
  328.3 1.0 copy-start.5
Sparse Core Ops, SparseCore 0:
  10.7 203.5 all-gather.1

commit v3 on v1

--- a/solution.py
+++ b/solution.py
@@ -35,8 +35,8 @@
     return exchange(copies, axis, groups)
 
 
-def far_groups(n):
-    return [list(range(i, n, NEAR)) for i in range(NEAR)]
+def far_groups(n, stride=NEAR):
+    return [list(range(i, n, stride)) for i in range(stride)]
 
 
 def chip_groups(n):
@@ -96,7 +96,14 @@
     total = keep.astype(f32) + ahead.astype(f32) + behind.astype(f32)
     total = total + jnp.concatenate([low, high], axis=0).astype(f32)
 
-    got = exchange(total.astype(BF16), "fs", far_groups(n))
+    blocks = total.astype(BF16).reshape(far // 2, 2, rows, width)
+    side = me // NEAR
+    keep, other = part_of(blocks, side, 1), part_of(blocks, side + 1, 1)
+    h = far // 4
+    low, high = shift(other[:h], NEAR), shift(other[h:], -NEAR)
+    total = keep.astype(f32) + jnp.concatenate([low, high], axis=0).astype(f32)
+
+    got = exchange(total.astype(BF16), "fs", far_groups(n, 2 * NEAR))
     return jnp.sum(got.astype(f32), axis=0)
 
 
@@ -161,7 +168,7 @@
 STEPS = 4
 
 
-def hidden_kernel(normed, whole):
+def hidden_kernel(normed, whole, copies):
     tokens, width = normed.shape
     planes, _, cols = whole.shape
     rows = width // planes
@@ -188,7 +195,9 @@
         def _():
             for m in range(halves):
                 gate, up = acc_ref[m], acc_ref[halves + m]
-                o_ref[:, m * cols : (m + 1) * cols] = (gate / (1.0 + jnp.exp(-gate)) * up).astype(BF16)
+                value = (gate / (1.0 + jnp.exp(-gate)) * up).astype(BF16)
+                for c in range(copies):
+                    o_ref[c, :, m * cols : (m + 1) * cols] = value
 
     return pl.pallas_call(
         body,
@@ -197,8 +206,8 @@
             pl.BlockSpec((tokens, width // STEPS), lambda i: (0, i)),
             pl.BlockSpec((per, 2 * halves * rows, cols), lambda i: (i, 0, 0)),
         ],
-        out_specs=pl.BlockSpec((tokens, halves * cols), lambda i: (0, 0)),
-        out_shape=jax.ShapeDtypeStruct((tokens, halves * cols), BF16),
+        out_specs=pl.BlockSpec((copies, tokens, halves * cols), lambda i: (0, 0, 0)),
+        out_shape=jax.ShapeDtypeStruct((copies, tokens, halves * cols), BF16),
         scratch_shapes=[pltpu.VMEM((2 * halves, tokens, cols), jnp.float32)],
         name="hidden_second",
     )(normed, whole)
@@ -258,7 +267,8 @@
     d1, d2 = down_first.astype(BF16), down_second.astype(BF16)
 
     pack = [m[:, k * dcols : (k + 1) * dcols] for m in (g2, u2) for k in range(half)] + [d2]
-    whole = lax.all_gather(row_major(jnp.concatenate(pack, axis=0)), "fs", axis=0, tiled=True)
+    pack = jnp.concatenate(pack, axis=0)
+    whole = lax.all_gather(row_major(pack), "fs", axis=0, tiled=True)
     whole = row_major(whole).reshape(n_fs, 2 * half * rows + hid, dcols)
 
     r = rows // n_tp
@@ -299,9 +309,9 @@
     own = own + 0.5 * scatter_sum(partial)
 
     normed = spread_copies(normed_of(own), "tp", n_tp).reshape(n_tp * tokens, width)
-    hidden = hidden_kernel(normed, whole)
+    hidden = hidden_kernel(normed, whole, n_tp)
     step1, step2, step3, step4 = cast_in_plane(whole, rows)
-    hidden = spread_copies(hidden, "tp", n_tp)
+    hidden = exchange(hidden, "tp")
     cast = step1()
     done = step2(cast)
     out = down_kernel(hidden, whole, hid)

time: 359 us -> 351 us (0.978)
  the two profiles are of different devices: /device:TPU:36 before, /device:TPU:44 now
where the time goes in v3:
time: 351 us; the launch traced here: 350 us
  starting transfers between devices  134 us (38%)
  waiting for transfers between devices  126 us (36%)
  blocking collectives  36.6 us (10%)
  other arithmetic  16.6 us (5%)
  between operations  14.9 us (4%)
  local copies, waits for them, and re-layouts  11.8 us (3%)
  Pallas kernels  7.96 us (2%)
    all_to_all x5, waiting for transfers between devices, exchange(): lax.all_to_all(blocks, axis, split_axis=0, concat_axis=0, tiled=True, axi...  91.5 us
    all_to_all x5, starting transfers between devices, exchange(): lax.all_to_all(blocks, axis, split_axis=0, concat_axis=0, tiled=True, axi...  79.1 us
    all_to_all x3, blocking collectives, exchange(): lax.all_to_all(blocks, axis, split_axis=0, concat_axis=0, tiled=True, axi...  36.6 us
    ppermute x10, starting transfers between devices, shift(): return lax.ppermute(array, 'fs', [(i, (i + steps) % n) for i in range(n)])  33.2 us
    ppermute x10, waiting for transfers between devices, shift(): return lax.ppermute(array, 'fs', [(i, (i + steps) % n) for i in range(n)])  33.1 us
    ppermute x3, starting transfers between devices, shift_tp(): return lax.ppermute(array, 'tp', [(i, (i + steps) % n) for i in range(n)])  11.2 us
  transfers between devices with their start and end apart: 26, of which 12 were waited for; matrix products, arithmetic and copies ran while one was open for 6% of the time, Pallas kernels for 2%

profile of v3, /device:TPU:44, one launch (start us, length us, event | category | flops | bytes accessed | tf_op | source)
XLA Modules:
  0.0 349.7 jit_solution(8848463724541948272)
XLA Ops:
  11.8 4.8 %all-to-all-start = ((bf16[8,2,8,512]{3,2,1,0:T(8,128)(2,1)}), bf16[8,2,8,512]{3,2,1,0:T(8,128)(2,1)S(1)}, u32[]{:S(2)}, u32[]{:S(2)}) async-start(bf16[8,2,8,512]{3,2,1,0:T(8,128)(2,1)} %maximum_bitcast_fusion.1), calls=%async_computation | async-start | bytes 262144 | tf_op jit(solution)/shard_map/all_to_all | solution.py:28
  16.6 3.4 all-to-all-done
  20.7 3.8 %collective-permute-start = (bf16[512,128]{1,0:T(8,128)(2,1)S(1)}, bf16[512,128]{1,0:T(8,128)(2,1)S(1)}, u32[]{:S(2)}, u32[]{:S(2)}) collective-permute-start(bf16[512,128]{1,0:T(8,128)(2,1)S(1)} %pad_maximum_fusion.4), channel_id=1, source_target_pairs={{0,6},{1,7},{2,0},{3,1},{4,2},{5,3},{6,4},{7,5},{8,14},{9,15},{10,... | collective-permute-start | bytes 393224 | tf_op jit(solution)/shard_map/ppermute | solution.py:57
  24.6 4.0 %collective-permute-start.1 = (bf16[512,128]{1,0:T(8,128)(2,1)S(1)}, bf16[512,128]{1,0:T(8,128)(2,1)S(1)}, u32[]{:S(2)}, u32[]{:S(2)}) collective-permute-start(bf16[512,128]{1,0:T(8,128)(2,1)S(1)} %pad_maximum_fusion.4), channel_id=1, source_target_pairs={{0,4},{1,5},{2,6},{3,7},{4,0},{5,1},{6,2},{7,3},{8,12},{9,13},{10,... | collective-permute-start | bytes 393224 | tf_op jit(solution)/shard_map/ppermute | solution.py:57
  28.6 3.4 collective-permute-start.2
  32.0 45.8 %all-to-all-start.1 = ((bf16[32,2,8,128]{3,2,1,0:T(8,128)(2,1)}), bf16[32,2,8,128]{3,2,1,0:T(8,128)(2,1)S(1)}, u32[]{:S(2)}, u32[]{:S(2)}) async-start(bf16[32,2,8,128]{3,2,1,0:T(8,128)(2,1)} %bitcast.3), calls=%async_computation.1 | async-start | bytes 262144 | tf_op jit(solution)/shard_map/all_to_all | solution.py:28
  78.0 2.0 collective-permute-start.3
  80.0 1.9 collective-permute-done.3
  82.1 27.8 %all-to-all-done.1 = bf16[32,2,8,128]{3,2,1,0:T(8,128)(2,1)S(1)} async-done(((bf16[32,2,8,128]{3,2,1,0:T(8,128)(2,1)}), bf16[32,2,8,128]{3,2,1,0:T(8,128)(2,1)S(1)}, u32[]{:S(2)}, u32[]{:S(2)}) %all-to-all-start.1) | async-done | bytes 131104 | tf_op jit(solution)/shard_map/all_to_all | solution.py:28
  109.9 10.0 %all_to_all.40 = bf16[4,512,128]{2,1,0:T(8,128)(2,1)S(1)} all-to-all(bf16[4,512,128]{2,1,0:T(8,128)(2,1)S(1)} %broadcast_in_dim.53), channel_id=1, replica_groups={{0,2,4,6},{1,3,5,7},{8,10,12,14},{9,11,13,15},{16,18,20,22},{17,19,21,2..., dimensions={0} | all-to-all | bytes 1048576 | tf_op jit(solution)/shard_map/all_to_all | solution.py:28
  119.9 1.9 collective-permute-start.4
  123.3 1.3 copy.36
  124.6 1.1 select_bitcast_fusion.1
  128.9 1.9 collective-permute-start.6
  130.8 4.0 %collective-permute-start.5 = (bf16[8,8,2048]{2,1,0:T(8,128)(2,1)S(1)}, bf16[8,8,2048]{2,1,0:T(8,128)(2,1)S(1)}, u32[]{:S(2)}, u32[]{:S(2)}) collective-permute-start(bf16[8,8,2048]{2,1,0:T(8,128)(2,1)S(1)} %get-tuple-element.36), channel_id=1, source_target_pairs={{0,8},{8,16},{16,24},{24,32},{32,40},{40,48},{48,56},{56,64},{64,7... | collective-permute-start | bytes 786440 | tf_op jit(solution)/shard_map/ppermute | solution.py:76
  135.5 2.4 collective-permute-start.8
  138.5 4.4 %collective-permute-start.7 = (bf16[4,8,2048]{2,1,0:T(8,128)(2,1)}, bf16[4,8,2048]{2,1,0:T(8,128)(2,1)}, u32[]{:S(2)}, u32[]{:S(2)}) collective-permute-start(bf16[4,8,2048]{2,1,0:T(8,128)(2,1)} %slice_bitcast_fusion.2), channel_id=1, source_target_pairs={{0,16},{8,24},{16,32},{24,40},{32,48},{40,56},{48,64},{56,72},{64,... | collective-permute-start | bytes 393224 | tf_op jit(solution)/shard_map/ppermute | solution.py:76
  143.0 9.3 %collective-permute-done.8 = bf16[4,8,2048]{2,1,0:T(8,128)(2,1)S(1)} collective-permute-done((bf16[4,8,2048]{2,1,0:T(8,128)(2,1)}, bf16[4,8,2048]{2,1,0:T(8,128)(2,1)S(1)}, u32[]{:S(2)}, u32[]{:S(2)}) %collective-permute-start.8) | collective-permute-done | bytes 131104 | tf_op jit(solution)/shard_map/ppermute | solution.py:76
  152.2 3.0 collective-permute-done.7
  156.3 2.8 collective-permute-start.10
  159.1 7.0 %collective-permute-start.9 = (bf16[2,8,2048]{2,1,0:T(8,128)(2,1)S(1)}, bf16[2,8,2048]{2,1,0:T(8,128)(2,1)S(1)}, u32[]{:S(2)}, u32[]{:S(2)}) collective-permute-start(bf16[2,8,2048]{2,1,0:T(8,128)(2,1)S(1)} %slice_bitcast_fusion.3), channel_id=1, source_target_pairs={{0,32},{8,40},{16,48},{24,56},{32,64},{40,72},{48,80},{56,88},{64,... | collective-permute-start | bytes 196616 | tf_op jit(solution)/shard_map/ppermute | solution.py:76
  166.2 4.1 %collective-permute-done.10 = bf16[2,8,2048]{2,1,0:T(8,128)(2,1)S(1)} collective-permute-done((bf16[2,8,2048]{2,1,0:T(8,128)(2,1)S(1)}, bf16[2,8,2048]{2,1,0:T(8,128)(2,1)S(1)}, u32[]{:S(2)}, u32[]{:S(2)}) %collective-permute-start.10) | collective-permute-done | bytes 65568 | tf_op jit(solution)/shard_map/ppermute | solution.py:76
  170.3 3.0 collective-permute-done.9
  174.0 7.6 %all-to-all-start.3 = ((bf16[4,8,2048]{2,1,0:T(8,128)(2,1)}), bf16[4,8,2048]{2,1,0:T(8,128)(2,1)S(1)}, u32[]{:S(2)}, u32[]{:S(2)}) async-start(bf16[4,8,2048]{2,1,0:T(8,128)(2,1)} %fusion.11), calls=%async_computation.3 | async-start | bytes 262144 | tf_op jit(solution)/shard_map/all_to_all | solution.py:28
  181.6 26.4 %all-to-all-done.3 = bf16[4,8,2048]{2,1,0:T(8,128)(2,1)S(1)} async-done(((bf16[4,8,2048]{2,1,0:T(8,128)(2,1)}), bf16[4,8,2048]{2,1,0:T(8,128)(2,1)S(1)}, u32[]{:S(2)}, u32[]{:S(2)}) %all-to-all-start.3) | async-done | bytes 131104 | tf_op jit(solution)/shard_map/all_to_all | solution.py:28
  208.2 2.0 dynamic-slice_select_fusion.1
  212.8 12.1 %all_to_all.41 = bf16[8,8,2048]{2,1,0:T(8,128)(2,1)} all-to-all(bf16[8,8,2048]{2,1,0:T(8,128)(2,1)S(1)} %broadcast_in_dim.54), channel_id=1, replica_groups=mesh['grp'=2,'fs'=32,'tp'=8] {'tp'}, dimensions={0} | all-to-all | bytes 524288 | tf_op jit(solution)/shard_map/all_to_all | solution.py:28
  224.9 4.4 %hidden_second.1 = bf16[8,64,512]{2,1,0:T(8,128)(2,1)} custom-call(bf16[64,2048]{1,0:T(8,128)(2,1)} %bitcast.128, bf16[32,384,256]{2,1,0:T(8,128)(2,1)} %bitcast.105), custom_call_target="tpu_custom_call" | custom-call | tf_op jit(solution)/shard_map/hidden_second/pallas_call | solution.py:202
  229.3 14.6 %all_to_all.42.h_ref = bf16[8,64,512]{2,1,0:T(8,128)(2,1)} all-to-all(bf16[8,64,512]{2,1,0:T(8,128)(2,1)} %hidden_second.1), channel_id=1, replica_groups=mesh['grp'=2,'fs'=32,'tp'=8] {'tp'}, dimensions={0} | all-to-all | bytes 1048576 | tf_op jit(solution)/shard_map/all_to_all | solution.py:28
  243.9 3.6 %down_second.1 = f32[64,256]{1,0:T(8,128)} custom-call(bf16[8,64,512]{2,1,0:T(8,128)(2,1)} %all_to_all.42.h_ref, bf16[32,384,256]{2,1,0:T(8,128)(2,1)} %bitcast.106), custom_call_target="tpu_custom_call" | custom-call | tf_op jit(solution)/shard_map/down_second/pallas_call | solution.py:234
  247.4 6.5 %all-to-all-start.6 = ((f32[8,8,256]{2,1,0:T(8,128)}), f32[8,8,256]{2,1,0:T(8,128)S(1)}, u32[]{:S(2)}, u32[]{:S(2)}) async-start(f32[8,8,256]{2,1,0:T(8,128)} %bitcast.133), calls=%async_computation.6 | async-start | bytes 131072 | tf_op jit(solution)/shard_map/all_to_all | solution.py:28
  253.9 3.1 all-to-all-done.6
  257.1 1.2 broadcast_select_fusion
  258.3 1.7 collective-permute-start.16
  260.0 1.6 collective-permute-start.17
  263.2 14.4 %all-to-all-start.7 = ((bf16[8,8,2048]{2,1,0:T(8,128)(2,1)}), bf16[8,8,2048]{2,1,0:T(8,128)(2,1)S(1)}, u32[]{:S(2)}, u32[]{:S(2)}) async-start(bf16[8,8,2048]{2,1,0:T(8,128)(2,1)} %broadcast_in_dim.55), calls=%async_computation.7 | async-start | bytes 524288 | tf_op jit(solution)/shard_map/all_to_all | solution.py:28
  278.6 1.4 copy.44
  281.0 1.4 select_select_fusion
  283.5 1.3 collective-permute-start.19
  284.8 1.3 collective-permute-start.18
  286.1 30.8 %all-to-all-done.7 = bf16[8,8,2048]{2,1,0:T(8,128)(2,1)S(1)} async-done(((bf16[8,8,2048]{2,1,0:T(8,128)(2,1)}), bf16[8,8,2048]{2,1,0:T(8,128)(2,1)S(1)}, u32[]{:S(2)}, u32[]{:S(2)}) %all-to-all-start.7) | async-done | bytes 262176 | tf_op jit(solution)/shard_map/all_to_all | solution.py:28
  316.9 2.2 collective-permute-start.13
  319.1 4.6 %collective-permute-start.12 = (bf16[4,8,2048]{2,1,0:T(8,128)(2,1)S(1)}, bf16[4,8,2048]{2,1,0:T(8,128)(2,1)S(1)}, u32[]{:S(2)}, u32[]{:S(2)}) collective-permute-start(bf16[4,8,2048]{2,1,0:T(8,128)(2,1)S(1)} %get-tuple-element.43), channel_id=1, source_target_pairs={{0,16},{8,24},{16,32},{24,40},{32,48},{40,56},{48,64},{56,72},{64,... | collective-permute-start | bytes 393224 | tf_op jit(solution)/shard_map/ppermute | solution.py:76
  323.7 2.0 collective-permute-start.11
  325.8 6.2 %collective-permute-done.11 = bf16[8,8,2048]{2,1,0:T(8,128)(2,1)S(1)} collective-permute-done((bf16[8,8,2048]{2,1,0:T(8,128)(2,1)S(1)}, bf16[8,8,2048]{2,1,0:T(8,128)(2,1)S(1)}, u32[]{:S(2)}, u32[]{:S(2)}) %collective-permute-start.11) | collective-permute-done | bytes 262176 | tf_op jit(solution)/shard_map/ppermute | solution.py:76
  332.0 1.9 collective-permute-start.14
  334.0 7.5 %collective-permute-done.14 = bf16[8,8,2048]{2,1,0:T(8,128)(2,1)S(1)} collective-permute-done((bf16[8,8,2048]{2,1,0:T(8,128)(2,1)S(1)}, bf16[8,8,2048]{2,1,0:T(8,128)(2,1)S(1)}, u32[]{:S(2)}, u32[]{:S(2)}) %collective-permute-start.14) | collective-permute-done | bytes 262176 | tf_op jit(solution)/shard_map/ppermute | solution.py:76
  341.6 1.3 broadcast_select_fusion.1
  (90 shorter events, 20.9 us)
Async XLA Ops:
  7.2 9.4 %copy-start.7 = (f32[128,256]{1,0:T(8,128)S(1)}, f32[128,256]{1,0:T(8,128)}, u32[]{:S(2)}) copy-start(f32[128,256]{1,0:T(8,128)} %param.13) | copy-start | bytes 393220
  7.2 201.0 %all-gather.2.cloned.1.call-start = ((), (), s32[]{:S(2)}) async-start(), calls=%async_computation.8 | async-start | bytes 6488064 | tf_op jit(solution)/shard_map/all_gather | solution.py:271
  9.3 0.7 copy-start.6
  11.8 8.2 %all-to-all-start = ((bf16[8,2,8,512]{3,2,1,0:T(8,128)(2,1)}), bf16[8,2,8,512]{3,2,1,0:T(8,128)(2,1)S(1)}, u32[]{:S(2)}, u32[]{:S(2)}) async-start(bf16[8,2,8,512]{3,2,1,0:T(8,128)(2,1)} %maximum_bitcast_fusion.1), calls=%async_computation | async-start | bytes 262144 | tf_op jit(solution)/shard_map/all_to_all | solution.py:28
  20.7 57.2 %collective-permute-start = (bf16[512,128]{1,0:T(8,128)(2,1)S(1)}, bf16[512,128]{1,0:T(8,128)(2,1)S(1)}, u32[]{:S(2)}, u32[]{:S(2)}) collective-permute-start(bf16[512,128]{1,0:T(8,128)(2,1)S(1)} %pad_maximum_fusion.4), channel_id=1, source_target_pairs={{0,6},{1,7},{2,0},{3,1},{4,2},{5,3},{6,4},{7,5},{8,14},{9,15},{10,... | collective-permute-start | bytes 393224 | tf_op jit(solution)/shard_map/ppermute | solution.py:57
  24.6 53.4 %collective-permute-start.1 = (bf16[512,128]{1,0:T(8,128)(2,1)S(1)}, bf16[512,128]{1,0:T(8,128)(2,1)S(1)}, u32[]{:S(2)}, u32[]{:S(2)}) collective-permute-start(bf16[512,128]{1,0:T(8,128)(2,1)S(1)} %pad_maximum_fusion.4), channel_id=1, source_target_pairs={{0,4},{1,5},{2,6},{3,7},{4,0},{5,1},{6,2},{7,3},{8,12},{9,13},{10,... | collective-permute-start | bytes 393224 | tf_op jit(solution)/shard_map/ppermute | solution.py:57
  28.6 49.4 %collective-permute-start.2 = (bf16[512,128]{1,0:T(8,128)(2,1)S(1)}, bf16[512,128]{1,0:T(8,128)(2,1)S(1)}, u32[]{:S(2)}, u32[]{:S(2)}) collective-permute-start(bf16[512,128]{1,0:T(8,128)(2,1)S(1)} %pad_maximum_fusion.4), channel_id=1, source_target_pairs={{0,2},{1,3},{2,4},{3,5},{4,6},{5,7},{6,0},{7,1},{8,10},{9,11},{10,... | collective-permute-start | bytes 393224 | tf_op jit(solution)/shard_map/ppermute | solution.py:57
  32.0 77.8 %all-to-all-start.1 = ((bf16[32,2,8,128]{3,2,1,0:T(8,128)(2,1)}), bf16[32,2,8,128]{3,2,1,0:T(8,128)(2,1)S(1)}, u32[]{:S(2)}, u32[]{:S(2)}) async-start(bf16[32,2,8,128]{3,2,1,0:T(8,128)(2,1)} %bitcast.3), calls=%async_computation.1 | async-start | bytes 262144 | tf_op jit(solution)/shard_map/all_to_all | solution.py:28
  78.0 3.8 %collective-permute-start.3 = (bf16[4,512,128]{2,1,0:T(8,128)(2,1)S(1)}, bf16[4,512,128]{2,1,0:T(8,128)(2,1)S(1)}, u32[]{:S(2)}, u32[]{:S(2)}) collective-permute-start(bf16[4,512,128]{2,1,0:T(8,128)(2,1)S(1)} %bitcast_dynamic-update-slice_fusion.3), channel_id=1, source_target_pairs={{0,1},{1,0},{2,3},{3,2},{4,5},{5,4},{6,7},{7,6},{8,9},{9,8},{10,11... | collective-permute-start | bytes 1572872 | tf_op jit(solution)/shard_map/ppermute | solution.py:68
  82.0 39.9 %copy-start = (bf16[256,2048]{1,0:T(8,128)(2,1)S(1)}, bf16[256,2048]{1,0:T(8,128)(2,1)}, u32[]{:S(2)}) copy-start(bf16[256,2048]{1,0:T(8,128)(2,1)} %param.9) | copy-start | bytes 3145732
  119.9 4.7 %collective-permute-start.4 = (bf16[4,512,128]{2,1,0:T(8,128)(2,1)S(1)}, bf16[4,512,128]{2,1,0:T(8,128)(2,1)}, u32[]{:S(2)}, u32[]{:S(2)}) collective-permute-start(bf16[4,512,128]{2,1,0:T(8,128)(2,1)S(1)} %all_to_all.40), channel_id=1, source_target_pairs={{0,1},{1,0},{2,3},{3,2},{4,5},{5,4},{6,7},{7,6},{8,9},{9,8},{10,11... | collective-permute-start | bytes 1572872 | tf_op jit(solution)/shard_map/ppermute | solution.py:49
  126.3 1.8 copy-start.3
  126.5 0.8 copy-start.5
  128.9 26.4 %collective-permute-start.6 = (bf16[8,8,2048]{2,1,0:T(8,128)(2,1)}, bf16[8,8,2048]{2,1,0:T(8,128)(2,1)S(1)}, u32[]{:S(2)}, u32[]{:S(2)}) collective-permute-start(bf16[8,8,2048]{2,1,0:T(8,128)(2,1)} %get-tuple-element.35), channel_id=1, source_target_pairs={{0,248},{8,0},{16,8},{24,16},{32,24},{40,32},{48,40},{56,48},{64,5... | collective-permute-start | bytes 786440 | tf_op jit(solution)/shard_map/ppermute | solution.py:76
  130.8 24.4 %collective-permute-start.5 = (bf16[8,8,2048]{2,1,0:T(8,128)(2,1)S(1)}, bf16[8,8,2048]{2,1,0:T(8,128)(2,1)S(1)}, u32[]{:S(2)}, u32[]{:S(2)}) collective-permute-start(bf16[8,8,2048]{2,1,0:T(8,128)(2,1)S(1)} %get-tuple-element.36), channel_id=1, source_target_pairs={{0,8},{8,16},{16,24},{24,32},{32,40},{40,48},{48,56},{56,64},{64,7... | collective-permute-start | bytes 786440 | tf_op jit(solution)/shard_map/ppermute | solution.py:76
  135.5 16.8 %collective-permute-start.8 = (bf16[4,8,2048]{2,1,0:T(8,128)(2,1)}, bf16[4,8,2048]{2,1,0:T(8,128)(2,1)S(1)}, u32[]{:S(2)}, u32[]{:S(2)}) collective-permute-start(bf16[4,8,2048]{2,1,0:T(8,128)(2,1)} %dynamic-slice_bitcast_fusion.3), channel_id=1, source_target_pairs={{0,240},{8,248},{16,0},{24,8},{32,16},{40,24},{48,32},{56,40},{64,... | collective-permute-start | bytes 393224 | tf_op jit(solution)/shard_map/ppermute | solution.py:76
  138.5 16.7 %collective-permute-start.7 = (bf16[4,8,2048]{2,1,0:T(8,128)(2,1)}, bf16[4,8,2048]{2,1,0:T(8,128)(2,1)}, u32[]{:S(2)}, u32[]{:S(2)}) collective-permute-start(bf16[4,8,2048]{2,1,0:T(8,128)(2,1)} %slice_bitcast_fusion.2), channel_id=1, source_target_pairs={{0,16},{8,24},{16,32},{24,40},{32,48},{40,56},{48,64},{56,72},{64,... | collective-permute-start | bytes 393224 | tf_op jit(solution)/shard_map/ppermute | solution.py:76
  156.3 14.0 %collective-permute-start.10 = (bf16[2,8,2048]{2,1,0:T(8,128)(2,1)S(1)}, bf16[2,8,2048]{2,1,0:T(8,128)(2,1)S(1)}, u32[]{:S(2)}, u32[]{:S(2)}) collective-permute-start(bf16[2,8,2048]{2,1,0:T(8,128)(2,1)S(1)} %dynamic-slice_bitcast_fusion.5), channel_id=1, source_target_pairs={{0,224},{8,232},{16,240},{24,248},{32,0},{40,8},{48,16},{56,24},{6... | collective-permute-start | bytes 196616 | tf_op jit(solution)/shard_map/ppermute | solution.py:76
  159.1 14.2 %collective-permute-start.9 = (bf16[2,8,2048]{2,1,0:T(8,128)(2,1)S(1)}, bf16[2,8,2048]{2,1,0:T(8,128)(2,1)S(1)}, u32[]{:S(2)}, u32[]{:S(2)}) collective-permute-start(bf16[2,8,2048]{2,1,0:T(8,128)(2,1)S(1)} %slice_bitcast_fusion.3), channel_id=1, source_target_pairs={{0,32},{8,40},{16,48},{24,56},{32,64},{40,72},{48,80},{56,88},{64,... | collective-permute-start | bytes 196616 | tf_op jit(solution)/shard_map/ppermute | solution.py:76
  174.0 34.0 %all-to-all-start.3 = ((bf16[4,8,2048]{2,1,0:T(8,128)(2,1)}), bf16[4,8,2048]{2,1,0:T(8,128)(2,1)S(1)}, u32[]{:S(2)}, u32[]{:S(2)}) async-start(bf16[4,8,2048]{2,1,0:T(8,128)(2,1)} %fusion.11), calls=%async_computation.3 | async-start | bytes 262144 | tf_op jit(solution)/shard_map/all_to_all | solution.py:28
  211.2 45.9 %collective-permute-start.15 = (bf16[2,2048,128]{2,1,0:T(8,128)(2,1)}, bf16[2,2048,128]{2,1,0:T(8,128)(2,1)S(1)}, u32[]{:S(2)}, u32[]{:S(2)}) collective-permute-start(bf16[2,2048,128]{2,1,0:T(8,128)(2,1)} %pad_maximum_fusion.2), channel_id=1, source_target_pairs={{0,1},{8,9},{16,17},{24,25},{33,32},{41,40},{49,48},{57,56},{66,67... | collective-permute-start | bytes 3145736 | tf_op jit(solution)/shard_map/ppermute | solution.py:143
  247.4 9.6 %all-to-all-start.6 = ((f32[8,8,256]{2,1,0:T(8,128)}), f32[8,8,256]{2,1,0:T(8,128)S(1)}, u32[]{:S(2)}, u32[]{:S(2)}) async-start(f32[8,8,256]{2,1,0:T(8,128)} %bitcast.133), calls=%async_computation.6 | async-start | bytes 131072 | tf_op jit(solution)/shard_map/all_to_all | solution.py:28
  257.1 20.5 %copy-start.1 = (bf16[2,2048,128]{2,1,0:T(8,128)(2,1)}, bf16[2,2048,128]{2,1,0:T(8,128)(2,1)S(1)}, u32[]{:S(2)}) copy-start(bf16[2,2048,128]{2,1,0:T(8,128)(2,1)S(1)} %collective-permute-done.15) | copy-start | bytes 3145732
  258.3 22.7 %collective-permute-start.16 = (bf16[2,2048,128]{2,1,0:T(8,128)(2,1)}, bf16[2,2048,128]{2,1,0:T(8,128)(2,1)}, u32[]{:S(2)}, u32[]{:S(2)}) collective-permute-start(bf16[2,2048,128]{2,1,0:T(8,128)(2,1)} %broadcast_select_fusion), channel_id=1, source_target_pairs={{0,2},{1,3},{8,10},{9,11},{16,18},{17,19},{24,26},{25,27},{32,34},... | collective-permute-start | bytes 3145736 | tf_op jit(solution)/shard_map/ppermute | solution.py:143
  260.0 21.0 %collective-permute-start.17 = (bf16[2,2048,128]{2,1,0:T(8,128)(2,1)}, bf16[2,2048,128]{2,1,0:T(8,128)(2,1)}, u32[]{:S(2)}, u32[]{:S(2)}) collective-permute-start(bf16[2,2048,128]{2,1,0:T(8,128)(2,1)} %broadcast_select_fusion), channel_id=1, source_target_pairs={{0,6},{1,7},{8,14},{9,15},{16,22},{17,23},{24,30},{25,31},{32,38},... | collective-permute-start | bytes 3145736 | tf_op jit(solution)/shard_map/ppermute | solution.py:143
  263.2 53.7 %all-to-all-start.7 = ((bf16[8,8,2048]{2,1,0:T(8,128)(2,1)}), bf16[8,8,2048]{2,1,0:T(8,128)(2,1)S(1)}, u32[]{:S(2)}, u32[]{:S(2)}) async-start(bf16[8,8,2048]{2,1,0:T(8,128)(2,1)} %broadcast_in_dim.55), calls=%async_computation.7 | async-start | bytes 524288 | tf_op jit(solution)/shard_map/all_to_all | solution.py:28
  278.6 2.4 copy-start.2
  283.5 58.1 %collective-permute-start.19 = (bf16[2048,128]{1,0:T(8,128)(2,1)}, bf16[2048,128]{1,0:T(8,128)(2,1)S(1)}, u32[]{:S(2)}, u32[]{:S(2)}) collective-permute-start(bf16[2048,128]{1,0:T(8,128)(2,1)} %get-tuple-element.32), channel_id=1, source_target_pairs={{6,4},{7,5},{14,12},{15,13},{22,20},{23,21},{30,28},{31,29},{38,36... | collective-permute-start | bytes 1572872 | tf_op jit(solution)/shard_map/ppermute | solution.py:143
  284.8 56.8 %collective-permute-start.18 = (bf16[2048,128]{1,0:T(8,128)(2,1)}, bf16[2048,128]{1,0:T(8,128)(2,1)S(1)}, u32[]{:S(2)}, u32[]{:S(2)}) collective-permute-start(bf16[2048,128]{1,0:T(8,128)(2,1)} %get-tuple-element.33), channel_id=1, source_target_pairs={{2,4},{3,5},{10,12},{11,13},{18,20},{19,21},{26,28},{27,29},{34,36... | collective-permute-start | bytes 1572872 | tf_op jit(solution)/shard_map/ppermute | solution.py:143
  316.9 17.1 %collective-permute-start.13 = (bf16[4,8,2048]{2,1,0:T(8,128)(2,1)S(1)}, bf16[4,8,2048]{2,1,0:T(8,128)(2,1)S(1)}, u32[]{:S(2)}, u32[]{:S(2)}) collective-permute-start(bf16[4,8,2048]{2,1,0:T(8,128)(2,1)S(1)} %get-tuple-element.44), channel_id=1, source_target_pairs={{0,240},{8,248},{16,0},{24,8},{32,16},{40,24},{48,32},{56,40},{64,... | collective-permute-start | bytes 393224 | tf_op jit(solution)/shard_map/ppermute | solution.py:76
  319.1 14.9 %collective-permute-start.12 = (bf16[4,8,2048]{2,1,0:T(8,128)(2,1)S(1)}, bf16[4,8,2048]{2,1,0:T(8,128)(2,1)S(1)}, u32[]{:S(2)}, u32[]{:S(2)}) collective-permute-start(bf16[4,8,2048]{2,1,0:T(8,128)(2,1)S(1)} %get-tuple-element.43), channel_id=1, source_target_pairs={{0,16},{8,24},{16,32},{24,40},{32,48},{40,56},{48,64},{56,72},{64,... | collective-permute-start | bytes 393224 | tf_op jit(solution)/shard_map/ppermute | solution.py:76
  323.7 8.3 %collective-permute-start.11 = (bf16[8,8,2048]{2,1,0:T(8,128)(2,1)S(1)}, bf16[8,8,2048]{2,1,0:T(8,128)(2,1)S(1)}, u32[]{:S(2)}, u32[]{:S(2)}) collective-permute-start(bf16[8,8,2048]{2,1,0:T(8,128)(2,1)S(1)} %all-to-all-done.7), channel_id=1, source_target_pairs={{0,248},{8,0},{16,8},{24,16},{32,24},{40,32},{48,40},{56,48},{64,5... | collective-permute-start | bytes 786440 | tf_op jit(solution)/shard_map/ppermute | solution.py:76
  332.0 9.5 %collective-permute-start.14 = (bf16[8,8,2048]{2,1,0:T(8,128)(2,1)S(1)}, bf16[8,8,2048]{2,1,0:T(8,128)(2,1)S(1)}, u32[]{:S(2)}, u32[]{:S(2)}) collective-permute-start(bf16[8,8,2048]{2,1,0:T(8,128)(2,1)S(1)} %all-to-all-done.7), channel_id=1, source_target_pairs={{0,8},{8,16},{16,24},{24,32},{32,40},{40,48},{48,56},{56,64},{64,7... | collective-permute-start | bytes 786440 | tf_op jit(solution)/shard_map/ppermute | solution.py:76
  341.5 1.3 copy-start.4
Sparse Core Ops, SparseCore 0:
  10.7 196.8 all-gather.1

commit v4 on v3

--- a/solution.py
+++ b/solution.py
@@ -117,7 +117,8 @@
     me = lax.axis_index("fs")
     far, rows, width = got.shape
     h = far // 2
-    ahead, behind = shift(got, -1), shift(got, 1)
+    ahead = shift(got, -1)
+    behind = shift(got, 1)
     low, high = shift(got[:h], 2), shift(got[h:], -2)
     out = jnp.zeros((far, NEAR, rows, width), got.dtype)
     pieces = (got, ahead, jnp.concatenate([low, high], axis=0), behind)
@@ -267,8 +268,7 @@
     d1, d2 = down_first.astype(BF16), down_second.astype(BF16)
 
     pack = [m[:, k * dcols : (k + 1) * dcols] for m in (g2, u2) for k in range(half)] + [d2]
-    pack = jnp.concatenate(pack, axis=0)
-    whole = lax.all_gather(row_major(pack), "fs", axis=0, tiled=True)
+    whole = lax.all_gather(row_major(jnp.concatenate(pack, axis=0)), "fs", axis=0, tiled=True)
     whole = row_major(whole).reshape(n_fs, 2 * half * rows + hid, dcols)
 
     r = rows // n_tp

time: 351 us -> 351 us (level)
  no operation moved by 1% of the time
where the time goes in v4:
time: 351 us; the launch traced here: 350 us
  starting transfers between devices  134 us (38%)
  waiting for transfers between devices  126 us (36%)
  blocking collectives  36.6 us (10%)
  other arithmetic  16.6 us (5%)
  between operations  14.9 us (4%)
  local copies, waits for them, and re-layouts  11.8 us (3%)
  Pallas kernels  7.96 us (2%)
    all_to_all x5, waiting for transfers between devices, exchange(): lax.all_to_all(blocks, axis, split_axis=0, concat_axis=0, tiled=True, axi...  91.5 us
    all_to_all x5, starting transfers between devices, exchange(): lax.all_to_all(blocks, axis, split_axis=0, concat_axis=0, tiled=True, axi...  79.1 us
    all_to_all x3, blocking collectives, exchange(): lax.all_to_all(blocks, axis, split_axis=0, concat_axis=0, tiled=True, axi...  36.6 us
    ppermute x10, starting transfers between devices, shift(): return lax.ppermute(array, 'fs', [(i, (i + steps) % n) for i in range(n)])  33.2 us
    ppermute x10, waiting for transfers between devices, shift(): return lax.ppermute(array, 'fs', [(i, (i + steps) % n) for i in range(n)])  33.1 us
    ppermute x3, starting transfers between devices, shift_tp(): return lax.ppermute(array, 'tp', [(i, (i + steps) % n) for i in range(n)])  11.2 us
  transfers between devices with their start and end apart: 26, of which 12 were waited for; matrix products, arithmetic and copies ran while one was open for 6% of the time, Pallas kernels for 2%

profile of v4, /device:TPU:44, one launch (start us, length us, event | category | flops | bytes accessed | tf_op | source)
XLA Modules:
  0.0 349.7 jit_solution(8848463724541948272)
XLA Ops:
  11.8 4.8 %all-to-all-start = ((bf16[8,2,8,512]{3,2,1,0:T(8,128)(2,1)}), bf16[8,2,8,512]{3,2,1,0:T(8,128)(2,1)S(1)}, u32[]{:S(2)}, u32[]{:S(2)}) async-start(bf16[8,2,8,512]{3,2,1,0:T(8,128)(2,1)} %maximum_bitcast_fusion.1), calls=%async_computation | async-start | bytes 262144 | tf_op jit(solution)/shard_map/all_to_all | solution.py:28
  16.6 3.4 all-to-all-done
  20.7 3.8 %collective-permute-start = (bf16[512,128]{1,0:T(8,128)(2,1)S(1)}, bf16[512,128]{1,0:T(8,128)(2,1)S(1)}, u32[]{:S(2)}, u32[]{:S(2)}) collective-permute-start(bf16[512,128]{1,0:T(8,128)(2,1)S(1)} %pad_maximum_fusion.4), channel_id=1, source_target_pairs={{0,6},{1,7},{2,0},{3,1},{4,2},{5,3},{6,4},{7,5},{8,14},{9,15},{10,... | collective-permute-start | bytes 393224 | tf_op jit(solution)/shard_map/ppermute | solution.py:57
  24.6 4.0 %collective-permute-start.1 = (bf16[512,128]{1,0:T(8,128)(2,1)S(1)}, bf16[512,128]{1,0:T(8,128)(2,1)S(1)}, u32[]{:S(2)}, u32[]{:S(2)}) collective-permute-start(bf16[512,128]{1,0:T(8,128)(2,1)S(1)} %pad_maximum_fusion.4), channel_id=1, source_target_pairs={{0,4},{1,5},{2,6},{3,7},{4,0},{5,1},{6,2},{7,3},{8,12},{9,13},{10,... | collective-permute-start | bytes 393224 | tf_op jit(solution)/shard_map/ppermute | solution.py:57
  28.6 3.4 collective-permute-start.2
  32.0 45.8 %all-to-all-start.1 = ((bf16[32,2,8,128]{3,2,1,0:T(8,128)(2,1)}), bf16[32,2,8,128]{3,2,1,0:T(8,128)(2,1)S(1)}, u32[]{:S(2)}, u32[]{:S(2)}) async-start(bf16[32,2,8,128]{3,2,1,0:T(8,128)(2,1)} %bitcast.3), calls=%async_computation.1 | async-start | bytes 262144 | tf_op jit(solution)/shard_map/all_to_all | solution.py:28
  78.0 2.0 collective-permute-start.3
  80.0 1.9 collective-permute-done.3
  82.1 27.8 %all-to-all-done.1 = bf16[32,2,8,128]{3,2,1,0:T(8,128)(2,1)S(1)} async-done(((bf16[32,2,8,128]{3,2,1,0:T(8,128)(2,1)}), bf16[32,2,8,128]{3,2,1,0:T(8,128)(2,1)S(1)}, u32[]{:S(2)}, u32[]{:S(2)}) %all-to-all-start.1) | async-done | bytes 131104 | tf_op jit(solution)/shard_map/all_to_all | solution.py:28
  109.9 10.0 %all_to_all.40 = bf16[4,512,128]{2,1,0:T(8,128)(2,1)S(1)} all-to-all(bf16[4,512,128]{2,1,0:T(8,128)(2,1)S(1)} %broadcast_in_dim.53), channel_id=1, replica_groups={{0,2,4,6},{1,3,5,7},{8,10,12,14},{9,11,13,15},{16,18,20,22},{17,19,21,2..., dimensions={0} | all-to-all | bytes 1048576 | tf_op jit(solution)/shard_map/all_to_all | solution.py:28
  119.9 1.9 collective-permute-start.4
  123.3 1.3 copy.36
  124.6 1.1 select_bitcast_fusion.1
  128.9 1.9 collective-permute-start.6
  130.8 4.0 %collective-permute-start.5 = (bf16[8,8,2048]{2,1,0:T(8,128)(2,1)S(1)}, bf16[8,8,2048]{2,1,0:T(8,128)(2,1)S(1)}, u32[]{:S(2)}, u32[]{:S(2)}) collective-permute-start(bf16[8,8,2048]{2,1,0:T(8,128)(2,1)S(1)} %get-tuple-element.36), channel_id=1, source_target_pairs={{0,8},{8,16},{16,24},{24,32},{32,40},{40,48},{48,56},{56,64},{64,7... | collective-permute-start | bytes 786440 | tf_op jit(solution)/shard_map/ppermute | solution.py:76
  135.5 2.4 collective-permute-start.8
  138.5 4.4 %collective-permute-start.7 = (bf16[4,8,2048]{2,1,0:T(8,128)(2,1)}, bf16[4,8,2048]{2,1,0:T(8,128)(2,1)}, u32[]{:S(2)}, u32[]{:S(2)}) collective-permute-start(bf16[4,8,2048]{2,1,0:T(8,128)(2,1)} %slice_bitcast_fusion.2), channel_id=1, source_target_pairs={{0,16},{8,24},{16,32},{24,40},{32,48},{40,56},{48,64},{56,72},{64,... | collective-permute-start | bytes 393224 | tf_op jit(solution)/shard_map/ppermute | solution.py:76
  143.0 9.3 %collective-permute-done.8 = bf16[4,8,2048]{2,1,0:T(8,128)(2,1)S(1)} collective-permute-done((bf16[4,8,2048]{2,1,0:T(8,128)(2,1)}, bf16[4,8,2048]{2,1,0:T(8,128)(2,1)S(1)}, u32[]{:S(2)}, u32[]{:S(2)}) %collective-permute-start.8) | collective-permute-done | bytes 131104 | tf_op jit(solution)/shard_map/ppermute | solution.py:76
  152.2 3.0 collective-permute-done.7
  156.3 2.8 collective-permute-start.10
  159.1 7.0 %collective-permute-start.9 = (bf16[2,8,2048]{2,1,0:T(8,128)(2,1)S(1)}, bf16[2,8,2048]{2,1,0:T(8,128)(2,1)S(1)}, u32[]{:S(2)}, u32[]{:S(2)}) collective-permute-start(bf16[2,8,2048]{2,1,0:T(8,128)(2,1)S(1)} %slice_bitcast_fusion.3), channel_id=1, source_target_pairs={{0,32},{8,40},{16,48},{24,56},{32,64},{40,72},{48,80},{56,88},{64,... | collective-permute-start | bytes 196616 | tf_op jit(solution)/shard_map/ppermute | solution.py:76
  166.2 4.1 %collective-permute-done.10 = bf16[2,8,2048]{2,1,0:T(8,128)(2,1)S(1)} collective-permute-done((bf16[2,8,2048]{2,1,0:T(8,128)(2,1)S(1)}, bf16[2,8,2048]{2,1,0:T(8,128)(2,1)S(1)}, u32[]{:S(2)}, u32[]{:S(2)}) %collective-permute-start.10) | collective-permute-done | bytes 65568 | tf_op jit(solution)/shard_map/ppermute | solution.py:76
  170.3 3.0 collective-permute-done.9
  174.0 7.6 %all-to-all-start.3 = ((bf16[4,8,2048]{2,1,0:T(8,128)(2,1)}), bf16[4,8,2048]{2,1,0:T(8,128)(2,1)S(1)}, u32[]{:S(2)}, u32[]{:S(2)}) async-start(bf16[4,8,2048]{2,1,0:T(8,128)(2,1)} %fusion.11), calls=%async_computation.3 | async-start | bytes 262144 | tf_op jit(solution)/shard_map/all_to_all | solution.py:28
  181.6 26.4 %all-to-all-done.3 = bf16[4,8,2048]{2,1,0:T(8,128)(2,1)S(1)} async-done(((bf16[4,8,2048]{2,1,0:T(8,128)(2,1)}), bf16[4,8,2048]{2,1,0:T(8,128)(2,1)S(1)}, u32[]{:S(2)}, u32[]{:S(2)}) %all-to-all-start.3) | async-done | bytes 131104 | tf_op jit(solution)/shard_map/all_to_all | solution.py:28
  208.2 2.0 dynamic-slice_select_fusion.1
  212.8 12.1 %all_to_all.41 = bf16[8,8,2048]{2,1,0:T(8,128)(2,1)} all-to-all(bf16[8,8,2048]{2,1,0:T(8,128)(2,1)S(1)} %broadcast_in_dim.54), channel_id=1, replica_groups=mesh['grp'=2,'fs'=32,'tp'=8] {'tp'}, dimensions={0} | all-to-all | bytes 524288 | tf_op jit(solution)/shard_map/all_to_all | solution.py:28
  224.9 4.4 %hidden_second.1 = bf16[8,64,512]{2,1,0:T(8,128)(2,1)} custom-call(bf16[64,2048]{1,0:T(8,128)(2,1)} %bitcast.128, bf16[32,384,256]{2,1,0:T(8,128)(2,1)} %bitcast.105), custom_call_target="tpu_custom_call" | custom-call | tf_op jit(solution)/shard_map/hidden_second/pallas_call | solution.py:203
  229.3 14.6 %all_to_all.42.h_ref = bf16[8,64,512]{2,1,0:T(8,128)(2,1)} all-to-all(bf16[8,64,512]{2,1,0:T(8,128)(2,1)} %hidden_second.1), channel_id=1, replica_groups=mesh['grp'=2,'fs'=32,'tp'=8] {'tp'}, dimensions={0} | all-to-all | bytes 1048576 | tf_op jit(solution)/shard_map/all_to_all | solution.py:28
  243.9 3.6 %down_second.1 = f32[64,256]{1,0:T(8,128)} custom-call(bf16[8,64,512]{2,1,0:T(8,128)(2,1)} %all_to_all.42.h_ref, bf16[32,384,256]{2,1,0:T(8,128)(2,1)} %bitcast.106), custom_call_target="tpu_custom_call" | custom-call | tf_op jit(solution)/shard_map/down_second/pallas_call | solution.py:235
  247.4 6.5 %all-to-all-start.6 = ((f32[8,8,256]{2,1,0:T(8,128)}), f32[8,8,256]{2,1,0:T(8,128)S(1)}, u32[]{:S(2)}, u32[]{:S(2)}) async-start(f32[8,8,256]{2,1,0:T(8,128)} %bitcast.133), calls=%async_computation.6 | async-start | bytes 131072 | tf_op jit(solution)/shard_map/all_to_all | solution.py:28
  253.9 3.1 all-to-all-done.6
  257.1 1.2 broadcast_select_fusion
  258.3 1.7 collective-permute-start.16
  260.0 1.6 collective-permute-start.17
  263.2 14.4 %all-to-all-start.7 = ((bf16[8,8,2048]{2,1,0:T(8,128)(2,1)}), bf16[8,8,2048]{2,1,0:T(8,128)(2,1)S(1)}, u32[]{:S(2)}, u32[]{:S(2)}) async-start(bf16[8,8,2048]{2,1,0:T(8,128)(2,1)} %broadcast_in_dim.55), calls=%async_computation.7 | async-start | bytes 524288 | tf_op jit(solution)/shard_map/all_to_all | solution.py:28
  278.6 1.4 copy.44
  281.0 1.4 select_select_fusion
  283.5 1.3 collective-permute-start.19
  284.8 1.3 collective-permute-start.18
  286.1 30.8 %all-to-all-done.7 = bf16[8,8,2048]{2,1,0:T(8,128)(2,1)S(1)} async-done(((bf16[8,8,2048]{2,1,0:T(8,128)(2,1)}), bf16[8,8,2048]{2,1,0:T(8,128)(2,1)S(1)}, u32[]{:S(2)}, u32[]{:S(2)}) %all-to-all-start.7) | async-done | bytes 262176 | tf_op jit(solution)/shard_map/all_to_all | solution.py:28
  316.9 2.2 collective-permute-start.13
  319.1 4.6 %collective-permute-start.12 = (bf16[4,8,2048]{2,1,0:T(8,128)(2,1)S(1)}, bf16[4,8,2048]{2,1,0:T(8,128)(2,1)S(1)}, u32[]{:S(2)}, u32[]{:S(2)}) collective-permute-start(bf16[4,8,2048]{2,1,0:T(8,128)(2,1)S(1)} %get-tuple-element.43), channel_id=1, source_target_pairs={{0,16},{8,24},{16,32},{24,40},{32,48},{40,56},{48,64},{56,72},{64,... | collective-permute-start | bytes 393224 | tf_op jit(solution)/shard_map/ppermute | solution.py:76
  323.7 2.0 collective-permute-start.11
  325.8 6.2 %collective-permute-done.11 = bf16[8,8,2048]{2,1,0:T(8,128)(2,1)S(1)} collective-permute-done((bf16[8,8,2048]{2,1,0:T(8,128)(2,1)S(1)}, bf16[8,8,2048]{2,1,0:T(8,128)(2,1)S(1)}, u32[]{:S(2)}, u32[]{:S(2)}) %collective-permute-start.11) | collective-permute-done | bytes 262176 | tf_op jit(solution)/shard_map/ppermute | solution.py:76
  332.0 1.9 collective-permute-start.14
  334.0 7.5 %collective-permute-done.14 = bf16[8,8,2048]{2,1,0:T(8,128)(2,1)S(1)} collective-permute-done((bf16[8,8,2048]{2,1,0:T(8,128)(2,1)S(1)}, bf16[8,8,2048]{2,1,0:T(8,128)(2,1)S(1)}, u32[]{:S(2)}, u32[]{:S(2)}) %collective-permute-start.14) | collective-permute-done | bytes 262176 | tf_op jit(solution)/shard_map/ppermute | solution.py:76
  341.6 1.3 broadcast_select_fusion.1
  (90 shorter events, 20.9 us)
Async XLA Ops:
  7.2 9.4 %copy-start.7 = (f32[128,256]{1,0:T(8,128)S(1)}, f32[128,256]{1,0:T(8,128)}, u32[]{:S(2)}) copy-start(f32[128,256]{1,0:T(8,128)} %param.13) | copy-start | bytes 393220
  7.2 201.0 %all-gather.2.cloned.1.call-start = ((), (), s32[]{:S(2)}) async-start(), calls=%async_computation.8 | async-start | bytes 6488064 | tf_op jit(solution)/shard_map/all_gather | solution.py:271
  9.3 0.7 copy-start.6
  11.8 8.2 %all-to-all-start = ((bf16[8,2,8,512]{3,2,1,0:T(8,128)(2,1)}), bf16[8,2,8,512]{3,2,1,0:T(8,128)(2,1)S(1)}, u32[]{:S(2)}, u32[]{:S(2)}) async-start(bf16[8,2,8,512]{3,2,1,0:T(8,128)(2,1)} %maximum_bitcast_fusion.1), calls=%async_computation | async-start | bytes 262144 | tf_op jit(solution)/shard_map/all_to_all | solution.py:28
  20.7 57.2 %collective-permute-start = (bf16[512,128]{1,0:T(8,128)(2,1)S(1)}, bf16[512,128]{1,0:T(8,128)(2,1)S(1)}, u32[]{:S(2)}, u32[]{:S(2)}) collective-permute-start(bf16[512,128]{1,0:T(8,128)(2,1)S(1)} %pad_maximum_fusion.4), channel_id=1, source_target_pairs={{0,6},{1,7},{2,0},{3,1},{4,2},{5,3},{6,4},{7,5},{8,14},{9,15},{10,... | collective-permute-start | bytes 393224 | tf_op jit(solution)/shard_map/ppermute | solution.py:57
  24.6 53.4 %collective-permute-start.1 = (bf16[512,128]{1,0:T(8,128)(2,1)S(1)}, bf16[512,128]{1,0:T(8,128)(2,1)S(1)}, u32[]{:S(2)}, u32[]{:S(2)}) collective-permute-start(bf16[512,128]{1,0:T(8,128)(2,1)S(1)} %pad_maximum_fusion.4), channel_id=1, source_target_pairs={{0,4},{1,5},{2,6},{3,7},{4,0},{5,1},{6,2},{7,3},{8,12},{9,13},{10,... | collective-permute-start | bytes 393224 | tf_op jit(solution)/shard_map/ppermute | solution.py:57
  28.6 49.4 %collective-permute-start.2 = (bf16[512,128]{1,0:T(8,128)(2,1)S(1)}, bf16[512,128]{1,0:T(8,128)(2,1)S(1)}, u32[]{:S(2)}, u32[]{:S(2)}) collective-permute-start(bf16[512,128]{1,0:T(8,128)(2,1)S(1)} %pad_maximum_fusion.4), channel_id=1, source_target_pairs={{0,2},{1,3},{2,4},{3,5},{4,6},{5,7},{6,0},{7,1},{8,10},{9,11},{10,... | collective-permute-start | bytes 393224 | tf_op jit(solution)/shard_map/ppermute | solution.py:57
  32.0 77.8 %all-to-all-start.1 = ((bf16[32,2,8,128]{3,2,1,0:T(8,128)(2,1)}), bf16[32,2,8,128]{3,2,1,0:T(8,128)(2,1)S(1)}, u32[]{:S(2)}, u32[]{:S(2)}) async-start(bf16[32,2,8,128]{3,2,1,0:T(8,128)(2,1)} %bitcast.3), calls=%async_computation.1 | async-start | bytes 262144 | tf_op jit(solution)/shard_map/all_to_all | solution.py:28
  78.0 3.8 %collective-permute-start.3 = (bf16[4,512,128]{2,1,0:T(8,128)(2,1)S(1)}, bf16[4,512,128]{2,1,0:T(8,128)(2,1)S(1)}, u32[]{:S(2)}, u32[]{:S(2)}) collective-permute-start(bf16[4,512,128]{2,1,0:T(8,128)(2,1)S(1)} %bitcast_dynamic-update-slice_fusion.3), channel_id=1, source_target_pairs={{0,1},{1,0},{2,3},{3,2},{4,5},{5,4},{6,7},{7,6},{8,9},{9,8},{10,11... | collective-permute-start | bytes 1572872 | tf_op jit(solution)/shard_map/ppermute | solution.py:68
  82.0 39.9 %copy-start = (bf16[256,2048]{1,0:T(8,128)(2,1)S(1)}, bf16[256,2048]{1,0:T(8,128)(2,1)}, u32[]{:S(2)}) copy-start(bf16[256,2048]{1,0:T(8,128)(2,1)} %param.9) | copy-start | bytes 3145732
  119.9 4.7 %collective-permute-start.4 = (bf16[4,512,128]{2,1,0:T(8,128)(2,1)S(1)}, bf16[4,512,128]{2,1,0:T(8,128)(2,1)}, u32[]{:S(2)}, u32[]{:S(2)}) collective-permute-start(bf16[4,512,128]{2,1,0:T(8,128)(2,1)S(1)} %all_to_all.40), channel_id=1, source_target_pairs={{0,1},{1,0},{2,3},{3,2},{4,5},{5,4},{6,7},{7,6},{8,9},{9,8},{10,11... | collective-permute-start | bytes 1572872 | tf_op jit(solution)/shard_map/ppermute | solution.py:49
  126.3 1.8 copy-start.3
  126.5 0.8 copy-start.5
  128.9 26.4 %collective-permute-start.6 = (bf16[8,8,2048]{2,1,0:T(8,128)(2,1)}, bf16[8,8,2048]{2,1,0:T(8,128)(2,1)S(1)}, u32[]{:S(2)}, u32[]{:S(2)}) collective-permute-start(bf16[8,8,2048]{2,1,0:T(8,128)(2,1)} %get-tuple-element.35), channel_id=1, source_target_pairs={{0,248},{8,0},{16,8},{24,16},{32,24},{40,32},{48,40},{56,48},{64,5... | collective-permute-start | bytes 786440 | tf_op jit(solution)/shard_map/ppermute | solution.py:76
  130.8 24.4 %collective-permute-start.5 = (bf16[8,8,2048]{2,1,0:T(8,128)(2,1)S(1)}, bf16[8,8,2048]{2,1,0:T(8,128)(2,1)S(1)}, u32[]{:S(2)}, u32[]{:S(2)}) collective-permute-start(bf16[8,8,2048]{2,1,0:T(8,128)(2,1)S(1)} %get-tuple-element.36), channel_id=1, source_target_pairs={{0,8},{8,16},{16,24},{24,32},{32,40},{40,48},{48,56},{56,64},{64,7... | collective-permute-start | bytes 786440 | tf_op jit(solution)/shard_map/ppermute | solution.py:76
  135.5 16.8 %collective-permute-start.8 = (bf16[4,8,2048]{2,1,0:T(8,128)(2,1)}, bf16[4,8,2048]{2,1,0:T(8,128)(2,1)S(1)}, u32[]{:S(2)}, u32[]{:S(2)}) collective-permute-start(bf16[4,8,2048]{2,1,0:T(8,128)(2,1)} %dynamic-slice_bitcast_fusion.3), channel_id=1, source_target_pairs={{0,240},{8,248},{16,0},{24,8},{32,16},{40,24},{48,32},{56,40},{64,... | collective-permute-start | bytes 393224 | tf_op jit(solution)/shard_map/ppermute | solution.py:76
  138.5 16.7 %collective-permute-start.7 = (bf16[4,8,2048]{2,1,0:T(8,128)(2,1)}, bf16[4,8,2048]{2,1,0:T(8,128)(2,1)}, u32[]{:S(2)}, u32[]{:S(2)}) collective-permute-start(bf16[4,8,2048]{2,1,0:T(8,128)(2,1)} %slice_bitcast_fusion.2), channel_id=1, source_target_pairs={{0,16},{8,24},{16,32},{24,40},{32,48},{40,56},{48,64},{56,72},{64,... | collective-permute-start | bytes 393224 | tf_op jit(solution)/shard_map/ppermute | solution.py:76
  156.3 14.0 %collective-permute-start.10 = (bf16[2,8,2048]{2,1,0:T(8,128)(2,1)S(1)}, bf16[2,8,2048]{2,1,0:T(8,128)(2,1)S(1)}, u32[]{:S(2)}, u32[]{:S(2)}) collective-permute-start(bf16[2,8,2048]{2,1,0:T(8,128)(2,1)S(1)} %dynamic-slice_bitcast_fusion.5), channel_id=1, source_target_pairs={{0,224},{8,232},{16,240},{24,248},{32,0},{40,8},{48,16},{56,24},{6... | collective-permute-start | bytes 196616 | tf_op jit(solution)/shard_map/ppermute | solution.py:76
  159.1 14.2 %collective-permute-start.9 = (bf16[2,8,2048]{2,1,0:T(8,128)(2,1)S(1)}, bf16[2,8,2048]{2,1,0:T(8,128)(2,1)S(1)}, u32[]{:S(2)}, u32[]{:S(2)}) collective-permute-start(bf16[2,8,2048]{2,1,0:T(8,128)(2,1)S(1)} %slice_bitcast_fusion.3), channel_id=1, source_target_pairs={{0,32},{8,40},{16,48},{24,56},{32,64},{40,72},{48,80},{56,88},{64,... | collective-permute-start | bytes 196616 | tf_op jit(solution)/shard_map/ppermute | solution.py:76
  174.0 34.0 %all-to-all-start.3 = ((bf16[4,8,2048]{2,1,0:T(8,128)(2,1)}), bf16[4,8,2048]{2,1,0:T(8,128)(2,1)S(1)}, u32[]{:S(2)}, u32[]{:S(2)}) async-start(bf16[4,8,2048]{2,1,0:T(8,128)(2,1)} %fusion.11), calls=%async_computation.3 | async-start | bytes 262144 | tf_op jit(solution)/shard_map/all_to_all | solution.py:28
  211.2 45.9 %collective-permute-start.15 = (bf16[2,2048,128]{2,1,0:T(8,128)(2,1)}, bf16[2,2048,128]{2,1,0:T(8,128)(2,1)S(1)}, u32[]{:S(2)}, u32[]{:S(2)}) collective-permute-start(bf16[2,2048,128]{2,1,0:T(8,128)(2,1)} %pad_maximum_fusion.2), channel_id=1, source_target_pairs={{0,1},{8,9},{16,17},{24,25},{33,32},{41,40},{49,48},{57,56},{66,67... | collective-permute-start | bytes 3145736 | tf_op jit(solution)/shard_map/ppermute | solution.py:144
  247.4 9.6 %all-to-all-start.6 = ((f32[8,8,256]{2,1,0:T(8,128)}), f32[8,8,256]{2,1,0:T(8,128)S(1)}, u32[]{:S(2)}, u32[]{:S(2)}) async-start(f32[8,8,256]{2,1,0:T(8,128)} %bitcast.133), calls=%async_computation.6 | async-start | bytes 131072 | tf_op jit(solution)/shard_map/all_to_all | solution.py:28
  257.1 20.5 %copy-start.1 = (bf16[2,2048,128]{2,1,0:T(8,128)(2,1)}, bf16[2,2048,128]{2,1,0:T(8,128)(2,1)S(1)}, u32[]{:S(2)}) copy-start(bf16[2,2048,128]{2,1,0:T(8,128)(2,1)S(1)} %collective-permute-done.15) | copy-start | bytes 3145732
  258.3 22.7 %collective-permute-start.16 = (bf16[2,2048,128]{2,1,0:T(8,128)(2,1)}, bf16[2,2048,128]{2,1,0:T(8,128)(2,1)}, u32[]{:S(2)}, u32[]{:S(2)}) collective-permute-start(bf16[2,2048,128]{2,1,0:T(8,128)(2,1)} %broadcast_select_fusion), channel_id=1, source_target_pairs={{0,2},{1,3},{8,10},{9,11},{16,18},{17,19},{24,26},{25,27},{32,34},... | collective-permute-start | bytes 3145736 | tf_op jit(solution)/shard_map/ppermute | solution.py:144
  260.0 21.0 %collective-permute-start.17 = (bf16[2,2048,128]{2,1,0:T(8,128)(2,1)}, bf16[2,2048,128]{2,1,0:T(8,128)(2,1)}, u32[]{:S(2)}, u32[]{:S(2)}) collective-permute-start(bf16[2,2048,128]{2,1,0:T(8,128)(2,1)} %broadcast_select_fusion), channel_id=1, source_target_pairs={{0,6},{1,7},{8,14},{9,15},{16,22},{17,23},{24,30},{25,31},{32,38},... | collective-permute-start | bytes 3145736 | tf_op jit(solution)/shard_map/ppermute | solution.py:144
  263.2 53.7 %all-to-all-start.7 = ((bf16[8,8,2048]{2,1,0:T(8,128)(2,1)}), bf16[8,8,2048]{2,1,0:T(8,128)(2,1)S(1)}, u32[]{:S(2)}, u32[]{:S(2)}) async-start(bf16[8,8,2048]{2,1,0:T(8,128)(2,1)} %broadcast_in_dim.55), calls=%async_computation.7 | async-start | bytes 524288 | tf_op jit(solution)/shard_map/all_to_all | solution.py:28
  278.6 2.4 copy-start.2
  283.5 58.1 %collective-permute-start.19 = (bf16[2048,128]{1,0:T(8,128)(2,1)}, bf16[2048,128]{1,0:T(8,128)(2,1)S(1)}, u32[]{:S(2)}, u32[]{:S(2)}) collective-permute-start(bf16[2048,128]{1,0:T(8,128)(2,1)} %get-tuple-element.32), channel_id=1, source_target_pairs={{6,4},{7,5},{14,12},{15,13},{22,20},{23,21},{30,28},{31,29},{38,36... | collective-permute-start | bytes 1572872 | tf_op jit(solution)/shard_map/ppermute | solution.py:144
  284.8 56.8 %collective-permute-start.18 = (bf16[2048,128]{1,0:T(8,128)(2,1)}, bf16[2048,128]{1,0:T(8,128)(2,1)S(1)}, u32[]{:S(2)}, u32[]{:S(2)}) collective-permute-start(bf16[2048,128]{1,0:T(8,128)(2,1)} %get-tuple-element.33), channel_id=1, source_target_pairs={{2,4},{3,5},{10,12},{11,13},{18,20},{19,21},{26,28},{27,29},{34,36... | collective-permute-start | bytes 1572872 | tf_op jit(solution)/shard_map/ppermute | solution.py:144
  316.9 17.1 %collective-permute-start.13 = (bf16[4,8,2048]{2,1,0:T(8,128)(2,1)S(1)}, bf16[4,8,2048]{2,1,0:T(8,128)(2,1)S(1)}, u32[]{:S(2)}, u32[]{:S(2)}) collective-permute-start(bf16[4,8,2048]{2,1,0:T(8,128)(2,1)S(1)} %get-tuple-element.44), channel_id=1, source_target_pairs={{0,240},{8,248},{16,0},{24,8},{32,16},{40,24},{48,32},{56,40},{64,... | collective-permute-start | bytes 393224 | tf_op jit(solution)/shard_map/ppermute | solution.py:76
  319.1 14.9 %collective-permute-start.12 = (bf16[4,8,2048]{2,1,0:T(8,128)(2,1)S(1)}, bf16[4,8,2048]{2,1,0:T(8,128)(2,1)S(1)}, u32[]{:S(2)}, u32[]{:S(2)}) collective-permute-start(bf16[4,8,2048]{2,1,0:T(8,128)(2,1)S(1)} %get-tuple-element.43), channel_id=1, source_target_pairs={{0,16},{8,24},{16,32},{24,40},{32,48},{40,56},{48,64},{56,72},{64,... | collective-permute-start | bytes 393224 | tf_op jit(solution)/shard_map/ppermute | solution.py:76
  323.7 8.3 %collective-permute-start.11 = (bf16[8,8,2048]{2,1,0:T(8,128)(2,1)S(1)}, bf16[8,8,2048]{2,1,0:T(8,128)(2,1)S(1)}, u32[]{:S(2)}, u32[]{:S(2)}) collective-permute-start(bf16[8,8,2048]{2,1,0:T(8,128)(2,1)S(1)} %all-to-all-done.7), channel_id=1, source_target_pairs={{0,248},{8,0},{16,8},{24,16},{32,24},{40,32},{48,40},{56,48},{64,5... | collective-permute-start | bytes 786440 | tf_op jit(solution)/shard_map/ppermute | solution.py:76
  332.0 9.5 %collective-permute-start.14 = (bf16[8,8,2048]{2,1,0:T(8,128)(2,1)S(1)}, bf16[8,8,2048]{2,1,0:T(8,128)(2,1)S(1)}, u32[]{:S(2)}, u32[]{:S(2)}) collective-permute-start(bf16[8,8,2048]{2,1,0:T(8,128)(2,1)S(1)} %all-to-all-done.7), channel_id=1, source_target_pairs={{0,8},{8,16},{16,24},{24,32},{32,40},{40,48},{48,56},{56,64},{64,7... | collective-permute-start | bytes 786440 | tf_op jit(solution)/shard_map/ppermute | solution.py:76
  341.5 1.3 copy-start.4
Sparse Core Ops, SparseCore 0:
  10.7 196.8 all-gather.1
